TPU v7x, 128 devices: a whole 4x4x4 slice. The times are simulated.
128 devices in a mesh: ep: 32 (over z, y, core), tp: 4 (over x).
Axes of the slice: x: 4, y: 4, z: 4, core: 2. Of those that a mesh axis runs over, the one named last changes fastest.
Arguments:
- tokens_first: bfloat16 [16384, 2048], P('ep'), may hold values from -6 to 6
- norm_gain_first: float32 [2048], replicated, may hold values from 0.1 to 1.9
- w_query: bfloat16 [2048, 512], P(None, 'tp'), may hold values from -0.125 to 0.125
- w_key: bfloat16 [2048, 512], P(None, 'tp'), may hold values from -0.125 to 0.125
- w_value: bfloat16 [2048, 1024], P(None, 'tp'), may hold values from -0.125 to 0.125
- w_outgate: bfloat16 [2048, 1024], P(None, 'tp'), may hold values from -0.125 to 0.125
- w_decay: bfloat16 [2048, 512], P(None, 'tp'), may hold values from -1 to 1
- decay_bias: float32 [256, 512], P('ep', 'tp'), may hold values from -1.3 to 12.5
- head_gain: float32 [1024], P('tp'), may hold values from 0.1 to 1.9
- w_mix_out: bfloat16 [1024, 2048], P('tp'), may hold values from -0.1875 to 0.1875
- tokens_second: bfloat16 [8192, 2048], P('ep'), may hold values from -6 to 6
- norm_gain_second: float32 [2048], replicated, may hold values from 0.1 to 1.9
- routes: int32 [8192, 2], P('ep'), may hold values from 0 to 31, all different within a row; in each aligned block of 256 rows (0 to 255, 256 to 511, ...) at most 32 rows name the same one
- route_logits: float32 [8192, 2], P('ep'), may hold values from -8 to 8
- expert_gate: bfloat16 [32, 2048, 3072], P('ep', None, 'tp'), may hold values from -0.125 to 0.125
- expert_up: bfloat16 [32, 2048, 3072], P('ep', None, 'tp'), may hold values from -0.125 to 0.125
- expert_down: bfloat16 [32, 3072, 2048], P('ep', 'tp'), may hold values from -0.109375 to 0.109375
Outputs:
- mixed_first: bfloat16 [16384, 2048], P(('ep', 'tp'))
- mixed_second: bfloat16 [8192, 2048], P('ep', 'tp')
Inputs may be any that keep to these rules, and one draw needn't show every extreme that they name: In the rows of one index of ep (aligned blocks of 256 rows) no expert is named by more than 32 rows, a bound that some block reaches; the two routes of a row name different experts.
All inputs are finite; a program needn't handle non-finite values.
Results may differ from a plain program's by a relative error of at most 0.01.
Values may be sent and summed in bfloat16 or wider, within the bound.
A program may use at most 128 MiB of HBM per device.

v0:
```python
import jax
import jax.numpy as jnp
from jax import lax
from jax.sharding import Mesh
from jax.sharding import PartitionSpec as P

KEY_DIM = 64
VALUE_DIM = 128
BLOCK = 64
EP = ("ep_0", "ep_1", "ep_2")
EP_TP = ("ep_0", "ep_1", "ep_2", "tp")


EPS = 1e-06
TEMPER = 16.0


def filled_with(shard, identity):
    return jax.tree.map(
        lambda a, e: jnp.broadcast_to(jnp.asarray(e, a.dtype), a.shape), shard, identity
    )


def all_in_one(shard, axis):
    leaves = jax.tree.leaves(shard)
    turns = sorted(range(len(leaves)), key=lambda k: -leaves[k].size)
    width = (1, *leaves[turns[0]].shape)[-1]
    lines = [
        jnp.pad(leaves[k].reshape(-1), (0, -leaves[k].size % width)).reshape(-1, width)
        for k in turns
    ]
    both, at, found = (lax.all_gather(jnp.concatenate(lines), axis), 0, {})
    for k, line in zip(turns, lines):
        share = both[:, at : at + len(line)].reshape(len(both), -1)
        found[k] = share[:, : leaves[k].size].reshape(-1, *leaves[k].shape)
        at += len(line)
    numbers = iter(range(len(leaves)))
    return jax.tree.map(lambda _: found[next(numbers)], shard)


def prefix_by_axis(shard, axes, combine, identity):
    before = start = filled_with(shard, identity)
    subtotal = shard
    for axis in reversed(axes):
        devices, place = (lax.axis_size(axis), lax.axis_index(axis))
        pieces = all_in_one(subtotal, axis)
        inside, subtotal = (start, start)
        for k in range(devices):
            passed = k < place
            subtotal = combine(subtotal, jax.tree.map(lambda part: part[k], pieces))
            inside = jax.tree.map(lambda new, old: jnp.where(passed, new, old), subtotal, inside)
        before = combine(inside, before)
    return before


def cut_along(shard, dim, devices):
    before, after = (shard.shape[:dim], shard.shape[dim + 1 :])
    return jnp.moveaxis(shard.reshape(*before, devices, -1, *after), dim, 0)


def summed_on_arrival(shard, axis, dim):
    devices = lax.axis_size(axis)
    pieces = lax.all_to_all(cut_along(shard, dim, devices), axis, 0, 0, tiled=True)
    return jnp.sum(pieces.astype(jnp.float32), axis=0)


def rms_rows(rows_in, gain_row):
    wide_rows = rows_in.astype(jnp.float32)
    return (
        wide_rows
        * lax.rsqrt(jnp.mean(wide_rows * wide_rows, axis=-1, keepdims=True) + EPS)
        * gain_row
    )


def block_step(entry_state, inputs):
    queries, key_rows, value_matrix_rows, log_decay = inputs
    cumul_log = jnp.cumsum(log_decay, axis=0)
    forward_decay_rows = queries * jnp.exp(cumul_log)
    behind = key_rows * jnp.exp(-cumul_log)
    scores = jnp.einsum("thk,shk->hts", forward_decay_rows, behind, precision=lax.Precision.HIGHEST)
    block_len = queries.shape[0]
    causal = jnp.arange(block_len)[:, None] >= jnp.arange(block_len)[None, :]
    scores = jnp.where(causal[None], scores, jnp.zeros_like(scores))
    within = jnp.einsum("hts,shv->thv", scores, value_matrix_rows, precision=lax.Precision.HIGHEST)
    carried_state = jnp.einsum(
        "azm,zmj->azj", forward_decay_rows, entry_state, precision=lax.Precision.HIGHEST
    )
    final_log_decay = cumul_log[-1]
    fading_factor = key_rows * jnp.exp(final_log_decay[None] - cumul_log)
    following_state = jnp.exp(final_log_decay)[:, :, None] * entry_state + jnp.einsum(
        "drx,drm->rxm", fading_factor, value_matrix_rows, precision=lax.Precision.HIGHEST
    )
    return (following_state, within + carried_state)


def head_output(attended, out_gate, head_gain):
    scaled = attended * lax.rsqrt(jnp.mean(attended * attended, axis=-1, keepdims=True) + EPS)
    return (scaled.reshape(attended.shape[0], -1) * head_gain * jax.nn.silu(out_gate)).astype(
        jnp.bfloat16
    )


def chain_join(earlier, later):
    return (earlier[0] * later[0], later[0][:, :, None] * earlier[1] + later[1])


def body(
    tokens_first,
    norm_gain_first,
    w_query,
    w_key,
    w_value,
    w_outgate,
    w_decay,
    decay_bias,
    head_gain,
    w_mix_out,
    tokens_second,
    norm_gain_second,
    routes,
    route_logits,
    expert_gate,
    expert_up,
    expert_down,
):
    ep_count = lax.axis_size(EP)
    normed = rms_rows(tokens_first, norm_gain_first).astype(jnp.bfloat16)
    first_rows = normed.shape[0]
    blocks = first_rows // BLOCK
    heads_here = w_query.shape[1] // KEY_DIM
    queries = (
        jnp.dot(normed, w_query, preferred_element_type=jnp.float32) * KEY_DIM ** (-0.5)
    ).astype(jnp.bfloat16)
    key_rows = jnp.dot(normed, w_key, preferred_element_type=jnp.float32).astype(jnp.bfloat16)
    value_matrix_rows = jnp.dot(normed, w_value, preferred_element_type=jnp.float32).astype(
        jnp.bfloat16
    )
    out_gate = jnp.dot(normed, w_outgate, preferred_element_type=jnp.float32)
    decay_pre = (
        jnp.dot(normed, w_decay, preferred_element_type=jnp.float32).reshape(blocks, BLOCK, -1)
        + decay_bias[:, None, :]
    )
    log_decay = (jax.nn.log_sigmoid(decay_pre) / TEMPER).reshape(blocks, BLOCK, heads_here, KEY_DIM)
    queries, key_rows, value_matrix_rows = lax.optimization_barrier(
        (queries, key_rows, value_matrix_rows)
    )
    query_wide = queries.astype(jnp.float32).reshape(blocks, BLOCK, heads_here, KEY_DIM)
    key_wide = key_rows.astype(jnp.float32).reshape(blocks, BLOCK, heads_here, KEY_DIM)
    value_wide = value_matrix_rows.astype(jnp.float32).reshape(blocks, BLOCK, heads_here, VALUE_DIM)
    start_state = jnp.zeros((heads_here, KEY_DIM, VALUE_DIM), jnp.float32)
    end_state, local_out = lax.scan(
        block_step, start_state, (query_wide, key_wide, value_wide, log_decay)
    )
    fade_total = jnp.exp(jnp.sum(log_decay, axis=(0, 1)))
    _, incoming_state = prefix_by_axis(
        (fade_total, end_state),
        EP,
        chain_join,
        (jnp.ones_like(fade_total), jnp.zeros_like(end_state)),
    )
    reach_log = jnp.cumsum(log_decay.reshape(first_rows, heads_here, KEY_DIM), axis=0)
    forward_decay_full = query_wide.reshape(first_rows, heads_here, KEY_DIM) * jnp.exp(reach_log)
    carried_state = jnp.einsum(
        "azm,zmj->azj", forward_decay_full, incoming_state, precision=lax.Precision.HIGHEST
    )
    attended = local_out.reshape(first_rows, heads_here, VALUE_DIM) + carried_state
    gated_rows = head_output(attended, out_gate, head_gain)
    spread = lax.all_to_all(gated_rows, "tp", split_axis=0, concat_axis=1, tiled=True)
    whole_out = lax.all_gather(w_mix_out, "tp", axis=0, tiled=True)
    mixed_first = jnp.dot(spread, whole_out, preferred_element_type=jnp.float32).astype(
        jnp.bfloat16
    )
    normed_second = rms_rows(tokens_second, norm_gain_second).astype(jnp.bfloat16)
    second_rows, model_width = normed_second.shape
    route_count = routes.shape[1]
    experts_all = ep_count * expert_gate.shape[0]
    slot_room = 2 * route_count * second_rows // experts_all
    flat_routes = routes.reshape(-1)
    member = (flat_routes[:, None] == jnp.arange(experts_all, dtype=jnp.int32)[None, :]).astype(
        jnp.int32
    )
    slot_index = jnp.sum((jnp.cumsum(member, axis=0) - 1) * member, axis=1)
    target = flat_routes * slot_room + slot_index
    copy_rows = jnp.repeat(normed_second, route_count, axis=0)
    buffer = (
        jnp.zeros((experts_all * slot_room, model_width), jnp.bfloat16).at[target].set(copy_rows)
    )
    buffer = buffer.reshape(experts_all, slot_room, model_width)
    arrived = lax.all_to_all(buffer, EP, split_axis=0, concat_axis=0, tiled=True)
    flat_rows = arrived.reshape(-1, model_width)
    gate_out = jnp.dot(flat_rows, expert_gate[0], preferred_element_type=jnp.float32)
    up_out = jnp.dot(flat_rows, expert_up[0], preferred_element_type=jnp.float32)
    hidden = (jax.nn.silu(gate_out) * up_out).astype(jnp.bfloat16)
    partial_value = jnp.dot(hidden, expert_down[0], preferred_element_type=jnp.float32)
    partial_value = partial_value.reshape(arrived.shape[0], arrived.shape[1], model_width)
    summed = summed_on_arrival(partial_value.astype(jnp.bfloat16), "tp", 2)
    returned = lax.all_to_all(
        summed.astype(jnp.bfloat16), EP, split_axis=0, concat_axis=0, tiled=True
    )
    received = returned.reshape(experts_all * slot_room, -1)
    picked = (
        jnp.take(received, target, axis=0).reshape(second_rows, route_count, -1).astype(jnp.float32)
    )
    route_share = jax.nn.sigmoid(route_logits - route_logits[:, ::-1])
    mixed_second = jnp.sum(picked * route_share[:, :, None], axis=1).astype(jnp.bfloat16)
    return (mixed_first, mixed_second)


def solution(mesh):
    split = Mesh(mesh.devices.reshape(4, 4, 2, mesh.shape["tp"]), ("ep_0", "ep_1", "ep_2", "tp"))
    in_specs = (
        P(EP, None),
        P(),
        P(None, "tp"),
        P(None, "tp"),
        P(None, "tp"),
        P(None, "tp"),
        P(None, "tp"),
        P(EP, "tp"),
        P("tp"),
        P("tp", None),
        P(EP, None),
        P(),
        P(EP, None),
        P(EP, None),
        P(EP, None, "tp"),
        P(EP, None, "tp"),
        P(EP, "tp", None),
    )
    out_specs = (P(EP_TP, None), P(EP, "tp"))
    return jax.shard_map(body, mesh=split, in_specs=in_specs, out_specs=out_specs, check_vma=False)
```

profile of v0, /device:TPU:1, one launch (start us, length us, event | category | flops | bytes accessed | tf_op | source)
XLA Modules:
  0.0 225.1 jit_solution(15726192445753947058)
XLA Ops:
  7.9 1.0 copy.115
  9.9 1.2 reduce-window.16
  11.6 1.5 fusion.23
  13.2 1.5 fusion.25
  14.7 2.6 %broadcast_in_dim.54 = bf16[256,2,2048]{2,1,0:T(2,128)(2,1)} broadcast(bf16[256,2048]{1,0:T(8,128)(2,1)S(1)} %fusion.25), dimensions={0,2} | broadcast | bytes 3145728 | tf_op jit(solution)/shard_map/broadcast_in_dim | solution.py:185
  17.3 4.1 %reshape.430 = bf16[512,2048]{1,0:T(8,128)(2,1)} reshape(bf16[256,2,2048]{2,1,0:T(2,128)(2,1)} %broadcast_in_dim.54) | data formatting | bytes 4194304 | tf_op jit(solution)/shard_map/reshape | solution.py:185
  21.6 7.5 %scatter_custom_fusion = bf16[1024,2048]{1,0:T(8,128)(2,1)} fusion(s32[512]{0:T(512)S(1)} %bitcast.238, bf16[512,2048]{1,0:T(8,128)(2,1)} %reshape.430, bf16[]{:T(256)} %constant.101.clone.1), kind=kCustom, calls=%fused_computation.47 | custom fusion | bytes 4194816 | tf_op jit(solution)/shard_map/scatter | solution.py:187
  29.1 9.8 %all-to-all-start.1 = ((bf16[32,32,2048]{2,1,0:T(8,128)(2,1)}), bf16[32,32,2048]{2,1,0:T(8,128)(2,1)}, u32[]{:S(2)}, u32[]{:S(2)}) async-start(bf16[32,32,2048]{2,1,0:T(8,128)(2,1)} %bitcast.216), calls=%async_computation.1 | async-start | bytes 8388608 | tf_op jit(solution)/shard_map/all_to_all | solution.py:190
  38.9 2.3 %fusion.13 = f32[512]{0:T(512)S(1)} fusion(bf16[512,2048]{1,0:T(8,128)(2,1)} %param.19), kind=kLoop, calls=%fused_computation.30 | loop fusion | flops 3145216 | bytes 2099200 | tf_op jit(solution)/shard_map/reduce_sum | solution.py:71
  41.8 1.4 convolution_convert_fusion.2
  44.7 1.1 reshape.400
  45.8 1.1 reshape.415
  46.9 2.0 reshape.417
  49.2 1.0 add.190.clone
  50.2 1.9 add.193
  52.1 3.3 %fusion.34 = (f32[128]{0:T(128)S(1)}, f32[512,128]{0,1:T(8,128)}) fusion(f32[512,128]{0,1:T(8,128)} %add.193, bf16[512,2048]{1,0:T(8,128)(2,1)} %copy-done.2, bf16[2048,128]{1,0:T(8,128)(2,1)} %param.25), kind=kOutput, calls=%fused_computation.66 | convolution fusion | flops 269156224 | bytes 3146240 | tf_op jit(solution)/shard_map/dot_general | solution.py:141
  55.4 1.9 reshape.395
  57.3 2.0 copy.101
  59.3 2.2 fusion.31
  61.5 35.1 %while.13 = (s32[]{:T(128)}, f32[2,64,128]{2,1,0:T(8,128)S(1)}, f32[8,64,2,128]{3,1,0,2:T(8,128)}, f32[8,64,2,64]{3,1,2,0:T(8,128)}, f32[8,64,2,64]{3,2,1,0:T(2,...) while((s32[]{:T(128)}, f32[2,64,128]{2,1,0:T(8,128)S(1)}, ...), condition=%wide.region_3.4_spmd.clone, body=%wide.region_1.3_spmd.clone.sunk | while | flops 44691456 | bytes 1191540 | solution.py:152
  62.4 1.0 bitcast_multiply_fusion.4
  66.8 1.0 bitcast_multiply_fusion.4
  71.2 1.0 bitcast_multiply_fusion.4
  80.0 1.0 bitcast_multiply_fusion.4
  93.1 1.0 bitcast_multiply_fusion.4
  96.6 1.7 copy.106
  98.5 2.2 all-gather.3
  100.8 6.3 %fusion.17 = f32[1024,768]{1,0:T(8,128)S(1)} fusion(bf16[1024,2048]{1,0:T(8,128)(2,1)} %bitcast.44, bf16[1,2048,768]{2,1,0:T(8,128)(2,1)} %param.34), kind=kOutput, calls=%fused_computation.36 | convolution fusion | flops 3221225472 | bytes 10485760 | tf_op jit(solution)/shard_map/dot_general | solution.py:193
  107.1 5.9 %multiply_convert_fusion = bf16[1024,768]{1,0:T(8,128)(2,1)S(1)} fusion(f32[1024,768]{1,0:T(8,128)S(1)} %fusion.17, bf16[1024,2048]{1,0:T(8,128)(2,1)} %bitcast.44, bf16[1,2048,768]{2,1,0:T(8,128)(2,1)S(1)} %copy-done.17), kind=kOutput, calls=%fused_computation.40 | convolution fusion | flops 3225944064 | bytes 12058624 | tf_op jit(solution)/shard_map/dot_general | solution.py:192
  113.0 3.6 %convolution_convert_fusion = bf16[32,32,2048]{2,1,0:T(8,128)(2,1)S(1)} fusion(bf16[32,32,768]{2,1,0:T(8,128)(2,1)S(1)} %bitcast.240, bf16[1,768,2048]{2,1,0:T(8,128)(2,1)S(1)} %copy-done), kind=kOutput, calls=%fused_computation.34 | convolution fusion | flops 3223322624 | bytes 8912896 | tf_op jit(solution)/shard_map/dot_general | solution.py:195
  116.7 2.6 %copy.161 = bf16[32,4,4,8,512]{4,3,1,0,2:T(8,128)(2,1)} copy(bf16[32,4,4,8,512]{4,3,2,1,0:T(8,128)(2,1)S(1)} %bitcast.219) | data formatting | bytes 8388608 | tf_op jit(solution)/shard_map/reshape | solution.py:58
  119.3 5.0 %all-to-all-start.2 = ((bf16[4,32,32,512]{3,2,1,0:T(8,128)(2,1)}), bf16[4,32,32,512]{3,2,1,0:T(8,128)(2,1)}, u32[]{:S(2)}, u32[]{:S(2)}) async-start(bf16[4,32,32,512]{3,2,1,0:T(8,128)(2,1)} %bitcast.217), calls=%async_computation.2 | async-start | bytes 8388608 | tf_op jit(solution)/shard_map/all_to_all | solution.py:63
  124.3 11.1 %all-gather.4 = f32[4,129,128]{2,1,0:T(8,128)S(1)} all-gather(f32[1,129,128]{2,1,0:T(8,128)S(1)} %maximum_bitcast_fusion.1), channel_id=3, replica_groups=mesh['ep_0'=4,'ep_1'=4,'ep_2'=2,'tp'=4] {'ep_1'}, dimensions={0}, use_global_device_ids=true | all-gather | bytes 330240 | tf_op jit(solution)/shard_map/all_gather | solution.py:32
  136.1 10.9 %all-gather.5 = f32[4,129,128]{2,1,0:T(8,128)S(1)} all-gather(f32[1,129,128]{2,1,0:T(8,128)S(1)} %maximum_bitcast_fusion.2), channel_id=4, replica_groups=mesh['ep_0'=4,'ep_1'=4,'ep_2'=2,'tp'=4] {'ep_0'}, dimensions={0}, use_global_device_ids=true | all-gather | bytes 330240 | tf_op jit(solution)/shard_map/all_gather | solution.py:32
  149.6 1.0 copy.112
  151.1 2.4 %reduce-window.14 = f32[64,2,4,128]{3,0,1,2:T(8,128)S(1)} reduce-window(f32[64,2,4,128]{3,0,1,2:T(8,128)S(1)} %copy_bitcast_fusion.5, f32[]{:T(128)} %constant.51.clone.1), window={size=1x1x1x128 pad=0_0x0_0x0_0x127_0}, to_apply=%region_5.6 | reduce-window | flops 8323072 | bytes 524292 | tf_op jit(solution)/shard_map/reduce-window
  154.0 2.3 %multiply_reduce_fusion.1 = (f32[512,2]{0,1:T(2,128)S(1)}, f32[512,2,128]{0,2,1:T(8,128)S(1)}) fusion(f32[512,2,128]{0,2,1:T(8,128)} %copy.112, f32[512,2,64]{0,2,1:T(8,128)} %bitcast.223, f32[2,64,128]{2,1,0:T(8,128)S(1)} %bitcast.227, f32[2,64,128]{2,1,0:T(8,128)S(1)} %bitcast.226, f32[2,64,128]{2,1,0:T(8,128)S(1)} %bitcast.235, ...), kind=kOutput, calls=%fused_computation.63 | convolution fusion | flops 101694464 | bytes 2240522 | tf_op jit(solution)/shard_map/azm,zmj->azj/dot_general | solution.py:164
  156.7 2.0 multiply_convert_fusion.1
  159.5 13.4 %all-to-all-done.2 = bf16[4,32,32,512]{3,2,1,0:T(8,128)(2,1)} async-done(((bf16[4,32,32,512]{3,2,1,0:T(8,128)(2,1)}), bf16[4,32,32,512]{3,2,1,0:T(8,128)(2,1)}, u32[]{:S(2)}, u32[]{:S(2)}) %all-to-all-start.2) | async-done | bytes 4194336 | tf_op jit(solution)/shard_map/all_to_all | solution.py:63
  172.9 3.4 %all-to-all-start = ((bf16[4,128,256]{1,2,0:T(8,128)(2,1)}), bf16[4,128,256]{1,2,0:T(8,128)(2,1)S(1)}, u32[]{:S(2)}, u32[]{:S(2)}) async-start(bf16[4,128,256]{1,2,0:T(8,128)(2,1)} %copy.114), calls=%async_computation | async-start | bytes 524288 | tf_op jit(solution)/shard_map/all_to_all | solution.py:169
  176.3 4.4 %reduce_sum.77 = bf16[32,32,512]{2,1,0:T(8,128)(2,1)} reduce(bf16[4,32,32,512]{3,2,1,0:T(8,128)(2,1)} %all-to-all-done.2, bf16[]{:T(256)} %constant.101.clone.1), dimensions={0}, to_apply=%region_13.14 | reduce | flops 1572864 | bytes 5242882 | tf_op jit(solution)/shard_map/reduce_sum | solution.py:64
  180.7 1.1 all-to-all-done
  181.8 9.3 %all-to-all-start.3 = ((bf16[32,32,512]{2,1,0:T(8,128)(2,1)}), bf16[32,32,512]{2,1,0:T(8,128)(2,1)}, u32[]{:S(2)}, u32[]{:S(2)}) async-start(bf16[32,32,512]{2,1,0:T(8,128)(2,1)} %reduce_sum.77), calls=%async_computation.3 | async-start | bytes 2097152 | tf_op jit(solution)/shard_map/all_to_all | solution.py:198
  191.9 3.7 %convolution_convert_fusion.1 = bf16[128,2048]{1,0:T(8,128)(2,1)} fusion(bf16[128,1024]{0,1:T(8,128)(2,1)S(1)} %bitcast.222, bf16[1024,2048]{1,0:T(8,128)(2,1)} %all-gather.8.cloned.1.call-done), kind=kOutput, calls=%fused_computation.43 | convolution fusion | flops 537133056 | bytes 4980736 | tf_op jit(solution)/shard_map/dot_general | solution.py:171
  195.6 12.6 %all-to-all-done.3 = bf16[32,32,512]{2,1,0:T(8,128)(2,1)} async-done(((bf16[32,32,512]{2,1,0:T(8,128)(2,1)}), bf16[32,32,512]{2,1,0:T(8,128)(2,1)}, u32[]{:S(2)}, u32[]{:S(2)}) %all-to-all-start.3) | async-done | bytes 1048608 | tf_op jit(solution)/shard_map/all_to_all | solution.py:198
  208.2 4.2 %gather_fusion = bf16[512,512]{1,0:T(8,128)(2,1)} fusion(bf16[1024,512]{1,0:T(8,128)(2,1)} %bitcast.51, s32[1024]{0:T(1024)S(1)} %pad_clamp_fusion), kind=kCustom, calls=%fused_computation | custom fusion | bytes 1050624 | tf_op jit(solution)/shard_map/jit(_take)/gather | solution.py:203
  212.4 2.0 gather.7
  214.4 3.9 %multiply_reduce_fusion = bf16[256,512]{1,0:T(8,128)(2,1)} fusion(bf16[256,2,512]{2,1,0:T(2,128)(2,1)} %gather.7, pred[256,2]{1,0:T(8,128)(4,1)S(1)} %copy.119, f32[256,2]{1,0:T(8,128)S(1)} %copy.122), kind=kLoop, calls=%fused_computation.56 | loop fusion | flops 917504 | bytes 788992 | tf_op jit(solution)/shard_map/reduce_sum | solution.py:206
  (193 shorter events, 40.4 us)
Async XLA Ops:
  7.2 105.9 %copy-start = (bf16[1,768,2048]{2,1,0:T(8,128)(2,1)S(1)}, bf16[1,768,2048]{2,1,0:T(8,128)(2,1)}, u32[]{:S(2)}) copy-start(bf16[1,768,2048]{2,1,0:T(8,128)(2,1)} %param.35) | copy-start | bytes 9437188
  7.2 184.7 %all-gather.8.cloned.1.call-start = ((), (), s32[]{:S(2)}) async-start(), calls=%async_computation.4 | async-start | bytes 5242880 | tf_op jit(solution)/shard_map/all_gather | solution.py:170
  29.1 12.1 %copy-start.11 = (f32[2048]{0:T(1024)S(1)}, f32[2048]{0:T(1024)}, u32[]{:S(2)}) copy-start(f32[2048]{0:T(1024)} %param.20) | copy-start | bytes 24580
  29.1 71.7 %all-to-all-start.1 = ((bf16[32,32,2048]{2,1,0:T(8,128)(2,1)}), bf16[32,32,2048]{2,1,0:T(8,128)(2,1)}, u32[]{:S(2)}, u32[]{:S(2)}) async-start(bf16[32,32,2048]{2,1,0:T(8,128)(2,1)} %bitcast.216), calls=%async_computation.1 | async-start | bytes 8388608 | tf_op jit(solution)/shard_map/all_to_all | solution.py:190
  38.9 2.3 %copy-start.4 = (bf16[512,2048]{1,0:T(8,128)(2,1)S(1)}, bf16[512,2048]{1,0:T(8,128)(2,1)}, u32[]{:S(2)}) copy-start(bf16[512,2048]{1,0:T(8,128)(2,1)} %param.19) | copy-start | bytes 6291460
  38.9 2.9 %copy-start.18 = (bf16[2048,256]{1,0:T(8,128)(2,1)S(1)}, bf16[2048,256]{1,0:T(8,128)(2,1)}, u32[]{:S(2)}) copy-start(bf16[2048,256]{1,0:T(8,128)(2,1)} %param.23) | copy-start | bytes 3145732
  41.2 2.0 copy-start.8
  41.8 2.2 copy-start.2
  41.8 2.2 copy-start.19
  43.2 5.7 %copy-start.10 = (f32[8,128]{1,0:T(8,128)S(1)}, f32[8,128]{1,0:T(8,128)}, u32[]{:S(2)}) copy-start(f32[8,128]{1,0:T(8,128)} %param.26) | copy-start | bytes 12292
  44.7 10.7 %copy-start.6 = (bf16[512,128]{1,0:T(8,128)(2,1)}, bf16[512,128]{1,0:T(8,128)(2,1)S(1)}, u32[]{:S(2)}) copy-start(bf16[512,128]{1,0:T(8,128)(2,1)S(1)} %fusion.29) | copy-start | bytes 393220
  100.8 6.3 %copy-start.17 = (bf16[1,2048,768]{2,1,0:T(8,128)(2,1)S(1)}, bf16[1,2048,768]{2,1,0:T(8,128)(2,1)}, u32[]{:S(2)}) copy-start(bf16[1,2048,768]{2,1,0:T(8,128)(2,1)} %param.33) | copy-start | bytes 9437188
  119.3 30.3 %copy-start.7 = (f32[8,64,2,128]{3,1,0,2:T(8,128)S(1)}, f32[8,64,2,128]{3,1,0,2:T(8,128)}, u32[]{:S(2)}) copy-start(f32[8,64,2,128]{3,1,0,2:T(8,128)} %get-tuple-element.46) | copy-start | bytes 1572868
  119.3 53.6 %all-to-all-start.2 = ((bf16[4,32,32,512]{3,2,1,0:T(8,128)(2,1)}), bf16[4,32,32,512]{3,2,1,0:T(8,128)(2,1)}, u32[]{:S(2)}, u32[]{:S(2)}) async-start(bf16[4,32,32,512]{3,2,1,0:T(8,128)(2,1)} %bitcast.217), calls=%async_computation.2 | async-start | bytes 8388608 | tf_op jit(solution)/shard_map/all_to_all | solution.py:63
  124.3 26.6 %copy-start.5 = (f32[512,128]{0,1:T(8,128)S(1)}, f32[512,128]{0,1:T(8,128)}, u32[]{:S(2)}) copy-start(f32[512,128]{0,1:T(8,128)} %get-tuple-element.157) | copy-start | bytes 786436
  135.6 18.3 %copy-start.13 = (f32[2,64]{1,0:T(2,128)}, f32[2,64]{1,0:T(2,128)S(1)}, u32[]{:S(2)}) copy-start(f32[2,64]{1,0:T(2,128)S(1)} %squeeze.89) | copy-start | bytes 1540
  135.7 18.2 %copy-start.14 = (f32[2,64]{1,0:T(2,128)}, f32[2,64]{1,0:T(2,128)S(1)}, u32[]{:S(2)}) copy-start(f32[2,64]{1,0:T(2,128)S(1)} %squeeze.90) | copy-start | bytes 1540
  135.8 18.2 %copy-start.15 = (f32[2,64]{1,0:T(2,128)}, f32[2,64]{1,0:T(2,128)S(1)}, u32[]{:S(2)}) copy-start(f32[2,64]{1,0:T(2,128)S(1)} %squeeze.91) | copy-start | bytes 1540
  135.9 18.1 %copy-start.16 = (f32[2,64]{1,0:T(2,128)}, f32[2,64]{1,0:T(2,128)S(1)}, u32[]{:S(2)}) copy-start(f32[2,64]{1,0:T(2,128)S(1)} %squeeze.93) | copy-start | bytes 1540
  153.7 3.0 %copy-start.3 = (bf16[512,2048]{1,0:T(8,128)(2,1)S(1)}, bf16[512,2048]{1,0:T(8,128)(2,1)}, u32[]{:S(2)}) copy-start(bf16[512,2048]{1,0:T(8,128)(2,1)} %copy-done.2) | copy-start | bytes 6291460
  153.8 2.8 %copy-start.20 = (f32[256]{0:T(256)S(1)}, f32[256]{0:T(256)}, u32[]{:S(2)}) copy-start(f32[256]{0:T(256)} %param.27) | copy-start | bytes 3076
  172.9 8.9 %all-to-all-start = ((bf16[4,128,256]{1,2,0:T(8,128)(2,1)}), bf16[4,128,256]{1,2,0:T(8,128)(2,1)S(1)}, u32[]{:S(2)}, u32[]{:S(2)}) async-start(bf16[4,128,256]{1,2,0:T(8,128)(2,1)} %copy.114), calls=%async_computation | async-start | bytes 524288 | tf_op jit(solution)/shard_map/all_to_all | solution.py:169
  176.3 15.0 %copy-start.9 = (s32[256,2]{0,1:T(2,128)S(1)}, s32[256,2]{0,1:T(2,128)}, u32[]{:S(2)}) copy-start(s32[256,2]{0,1:T(2,128)} %param.31) | copy-start | bytes 6148
  176.3 15.2 %copy-start.12 = (f32[256,2]{0,1:T(2,128)S(1)}, f32[256,2]{0,1:T(2,128)}, u32[]{:S(2)}) copy-start(f32[256,2]{0,1:T(2,128)} %param.32) | copy-start | bytes 6148
  181.8 26.4 %all-to-all-start.3 = ((bf16[32,32,512]{2,1,0:T(8,128)(2,1)}), bf16[32,32,512]{2,1,0:T(8,128)(2,1)}, u32[]{:S(2)}, u32[]{:S(2)}) async-start(bf16[32,32,512]{2,1,0:T(8,128)(2,1)} %reduce_sum.77), calls=%async_computation.3 | async-start | bytes 2097152 | tf_op jit(solution)/shard_map/all_to_all | solution.py:198
  208.2 10.1 %copy-start.1 = (bf16[1,768,2048]{2,1,0:T(8,128)(2,1)S(1)}, bf16[1,768,2048]{2,1,0:T(8,128)(2,1)}, u32[]{:S(2)}) copy-start(bf16[1,768,2048]{2,1,0:T(8,128)(2,1)} %param.35) | copy-start | bytes 9437188
Sparse Core Ops, SparseCore 0:
  9.7 51.1 all-gather.7
where the time goes:
time: 227 us; the launch traced here: 225 us
  local copies, waits for them, and re-layouts  58.1 us (26%)
  matrix products  42.5 us (19%)
  other arithmetic  29.8 us (13%)
  waiting for transfers between devices  27.9 us (12%)
  starting transfers between devices  27.5 us (12%)
  blocking collectives  24.2 us (11%)
  between operations  14.7 us (6%)
    all_gather x3, blocking collectives, all_in_one(): both, at, found = (lax.all_gather(jnp.concatenate(lines), axis), 0, {})  24.2 us
    dynamic_slice x16, local copies, waits for them, and re-layouts, body(): lax.scan(block_step, start_state, (query_wide, key_wide, value_wide, log_...  13.6 us
    all_to_all x1, waiting for transfers between devices, summed_on_arrival(): lax.all_to_all(cut_along(shard, dim, devices), axis, 0, 0, tiled=True)  13.4 us
    all_to_all x1, waiting for transfers between devices, body(): lax.all_to_all(summed.astype(jnp.bfloat16), EP, split_axis=0, concat_axis...  12.6 us
    all_to_all x1, starting transfers between devices, body(): lax.all_to_all(buffer, EP, split_axis=0, concat_axis=0, tiled=True)  9.79 us
    all_to_all x1, starting transfers between devices, body(): lax.all_to_all(summed.astype(jnp.bfloat16), EP, split_axis=0, concat_axis...  9.33 us
    mul x8, other arithmetic, block_step(): behind = key_rows * jnp.exp(-cumul_log)  7.9 us
    scatter x1, local copies, waits for them, and re-layouts, body(): jnp.zeros((experts_all * slot_room, model_width), jnp.bfloat16).at[target]  7.49 us
  transfers between devices with their start and end apart: 5, of which 3 were waited for; matrix products, arithmetic and copies ran while one was open for 53% of the time, Pallas kernels for 0%

commit v1 on v0

v1 whole, which is shorter than its diff:
```python
import jax
import jax.numpy as jnp
from jax import lax
from jax.experimental import pallas as pl
from jax.experimental.pallas import tpu as pltpu
from jax.sharding import PartitionSpec as P

KEY_DIM = 64
VALUE_DIM = 128
BLOCK = 64
CAP = 32
EPS = 1e-06
TEMPER = 16.0
NZ, NY, NC = 4, 4, 2
MESH = pl.DeviceIdType.MESH
HIGH = lax.Precision.HIGHEST
F32, BF16 = jnp.float32, jnp.bfloat16

ORDER = [
    (0, 0, 0), (0, 0, 1),
    (0, 1, 0), (1, 0, 0), (0, 3, 0), (3, 0, 0), (0, 2, 0), (2, 0, 0),
    (0, 1, 1), (1, 0, 1), (0, 3, 1), (3, 0, 1), (0, 2, 1), (2, 0, 1), (1, 1, 0), (3, 3, 0),
    (1, 3, 0), (3, 1, 0), (1, 1, 1), (3, 3, 1), (1, 2, 0), (2, 1, 0), (3, 2, 0), (2, 3, 0),
    (1, 3, 1), (3, 1, 1), (2, 2, 0), (1, 2, 1), (2, 1, 1), (3, 2, 1), (2, 3, 1), (2, 2, 1),
]
CHUNKS = 4
PER = 8


def dot(a, b, precision=None):
    return jnp.dot(a, b, preferred_element_type=F32, precision=precision)


def dot_t0(a, b, precision=None):
    return lax.dot_general(
        a, b, (((0,), (0,)), ((), ())), preferred_element_type=F32, precision=precision
    )


def dot_t1(a, b, precision=None):
    return lax.dot_general(
        a, b, (((1,), (1,)), ((), ())), preferred_element_type=F32, precision=precision
    )


def iota(shape, dim):
    return lax.broadcasted_iota(jnp.int32, shape, dim)


def rms(rows, gain):
    wide = rows.astype(F32)
    return wide * lax.rsqrt(jnp.mean(wide * wide, axis=-1, keepdims=True) + EPS) * gain


def log_sigmoid(x):
    return jnp.minimum(x, 0.0) - jnp.log1p(jnp.exp(-jnp.abs(x)))


def kernel(
    tok1_h, g1_ref, wq_h, wk_h, wv_h, wo_h, wd_h, bias_ref, hgain_ref, wmix_h,
    tok2_h, g2_ref, routes_ref, routes_t_ref, logits_ref, wg_h, wu_h, wdn_h,
    out1_ref, out2_ref,
    tok2, norm2, send2, recv2, tok1, norm1, w1, wmix, wg, wu, wdn, proj, att, reach,
    sbd, total, msg, pmsg, inc, joint, psend, prs, rsend, rret, mpart, mrecv, hid, chmsg, chrecv,
    ld, dsend, drecv, rs_ssem, rs_rsem, mx_ssem, mx_rsem, rt_ssem, rt_rsem,
    dd_ssem, dd_rsem, ch_ssem, ch_rsem,
):
    ep, tp = lax.axis_index("ep"), lax.axis_index("tp")
    z, y, c = ep // (NY * NC), (ep // NC) % NY, ep % NC
    chip = z * NY + y

    def target(o, sign=1):
        dz, dy, dc = o
        return (
            ((z + sign * dz + NZ) % NZ) * (NY * NC)
            + ((y + sign * dy + NY) % NY) * NC
            + (c + dc) % NC
        )

    def remote(src, dst, ssem, rsem, to_ep, to_tp):
        return pltpu.make_async_remote_copy(
            src_ref=src, dst_ref=dst, send_sem=ssem, recv_sem=rsem,
            device_id=(to_ep, to_tp), device_id_type=MESH,
        )

    loads = [
        (tok2_h, tok2), (tok1_h, tok1),
        (wq_h, w1.at[:, 0:128]), (wk_h, w1.at[:, 128:256]), (wv_h, w1.at[:, 256:512]),
        (wo_h, w1.at[:, 512:768]), (wd_h, w1.at[:, 768:896]),
        (wg_h.at[0], wg), (wu_h.at[0], wu), (wdn_h.at[0], wdn), (wmix_h, wmix),
    ]
    loads = [pltpu.make_async_copy(s, d, ld.at[i]) for i, (s, d) in enumerate(loads)]
    for cp in loads:
        cp.start()

    barrier = pltpu.get_barrier_semaphore()
    for o in ORDER[1:]:
        pl.semaphore_signal(barrier, inc=1, device_id=(target(o), tp), device_id_type=MESH)
    for d in range(1, 4):
        pl.semaphore_signal(barrier, inc=1, device_id=(ep, (tp + d) % 4), device_id_type=MESH)

    rows2 = norm2.shape[0]
    experts = send2.shape[0]
    r0t, r1t = routes_t_ref[0:1, :], routes_t_ref[1:2, :]
    e_sub = iota((experts, rows2), 0)
    member_t = ((r0t == e_sub) | (r1t == e_sub)).astype(F32)
    before_t = (iota((rows2, rows2), 0) < iota((rows2, rows2), 1)).astype(BF16)
    rank_t = dot(member_t.astype(BF16), before_t)
    place_t = jnp.where(member_t > 0.0, rank_t, -1.0)
    loads[0].wait()
    norm2[...] = rms(tok2[...], g2_ref[...]).astype(BF16)
    for g in range(experts // 8):
        place = place_t[8 * g : 8 * g + 8]
        want = iota((8, CAP, rows2), 1).astype(F32)
        pick = (place[:, None, :] == want).astype(BF16).reshape(8 * CAP, rows2)
        for n in range(norm2.shape[1] // 512):
            cols = slice(512 * n, 512 * n + 512)
            send2[8 * g : 8 * g + 8, :, cols] = (
                dot(pick, norm2[:, cols]).astype(BF16).reshape(8, CAP, 512)
            )
    pl.semaphore_wait(barrier, len(ORDER) - 1 + 3)

    def dispatch(s):
        to = target(ORDER[s])
        remote(send2.at[to], recv2.at[s], dsend, drecv.at[s // PER], to, tp).start()

    for s in range(1, 16):
        dispatch(s)
    recv2[0] = send2[ep]

    loads[1].wait()
    for i in range(tok1.shape[0] // 128):
        rows = slice(128 * i, 128 * i + 128)
        norm1[rows, :] = rms(tok1[rows, :], g1_ref[...]).astype(BF16)
    for i in range(2, 7):
        loads[i].wait()
    for lo, hi in ((0, 256), (256, 512), (512, 768), (768, 896)):
        proj[:, lo:hi] = dot(norm1[...], w1[:, lo:hi])
    sbd[...] = jnp.zeros_like(sbd)
    total[...] = jnp.zeros_like(total)
    own_head = (iota(sbd.shape, 0) // KEY_DIM == iota(sbd.shape, 1) // VALUE_DIM).astype(F32)
    tri = (iota((BLOCK, BLOCK), 0) >= iota((BLOCK, BLOCK), 1)).astype(F32)
    head_lane = iota((BLOCK, 2 * KEY_DIM), 1) // KEY_DIM

    def block(b, _):
        rows = pl.ds(pl.multiple_of(b * BLOCK, BLOCK), BLOCK)
        query = (proj[rows, 0:128] * KEY_DIM ** (-0.5)).astype(BF16).astype(F32)
        key = proj[rows, 128:256].astype(BF16).astype(F32)
        value = proj[rows, 256:512].astype(BF16).astype(F32)
        log_decay = log_sigmoid(proj[rows, 768:896] + bias_ref[pl.ds(b, 1), :]) / TEMPER
        cumul = dot(tri, log_decay, HIGH)
        final = cumul[BLOCK - 1 : BLOCK, :]
        forward = query * jnp.exp(cumul)
        behind = key * jnp.exp(-cumul)
        fading = key * jnp.exp(final - cumul)
        within = []
        for h in range(2):
            mine = jnp.where(head_lane == h, forward, 0.0)
            scores = dot_t1(mine, behind, HIGH)
            scores = jnp.where(tri > 0.0, scores, 0.0)
            within.append(dot(scores, value[:, VALUE_DIM * h : VALUE_DIM * (h + 1)], HIGH))
        att[rows, :] = jnp.concatenate(within, axis=1) + dot(forward, sbd[...], HIGH)
        fall = dot_t0(log_decay, jnp.ones((BLOCK, sbd.shape[1]), F32), HIGH)
        sbd[...] = jnp.exp(fall) * sbd[...] + own_head * dot_t0(fading, value, HIGH)
        reach[rows, :] = query * jnp.exp(cumul + total[0:1, :])
        total[0:1, :] = total[0:1, :] + final
        return 0

    lax.fori_loop(0, proj.shape[0] // BLOCK, block, 0)
    msg[0:64, :] = sbd[0:64, 0:128]
    msg[64:128, :] = sbd[64:128, 128:256]
    msg[128:136, :] = total[...]
    partner = ep + 1 - 2 * c
    first = remote(msg, pmsg, dd_ssem.at[0], dd_rsem.at[0], partner, tp)
    first.start()

    def column(row8):
        return jnp.exp(dot_t0(row8, jnp.ones((8, 128), F32), HIGH))

    def expert(j):
        x_rows = recv2[PER * j : PER * j + PER].reshape(PER * CAP, recv2.shape[2])
        for n in range(hid.shape[1] // 256):
            cols = slice(256 * n, 256 * n + 256)
            gate = dot(x_rows, wg[:, cols])
            up = dot(x_rows, wu[:, cols])
            hid[:, cols] = (gate * jax.nn.sigmoid(gate) * up).astype(BF16)
        for d in (1, 3, 2, 0):
            t = (tp + d) % 4
            cols = pl.ds(pl.multiple_of(t * 512, 512), 512)
            psend[j, d] = dot(hid[...], wdn[:, cols]).astype(BF16)
            if d:
                remote(psend.at[j, d], prs.at[j, d - 1], rs_ssem, rs_rsem.at[j], ep, t).start()

    def reduce(j):
        remote(prs.at[j], prs.at[j], rs_ssem, rs_rsem.at[j], ep, tp).wait_recv()
        whole = psend[j, 0].astype(F32)
        for d in range(3):
            whole = whole + prs[j, d].astype(F32)
        rsend[j] = whole.astype(BF16).reshape(PER, CAP, 512)
        for i in range(PER):
            s = PER * j + i
            if s == 0:
                rret[ep] = rsend[0, 0]
            else:
                to = target(ORDER[s], -1)
                remote(rsend.at[j, i], rret.at[ep], rt_ssem, rt_rsem, to, tp).start()

    def arrived(j):
        part = recv2.at[1:PER] if j == 0 else recv2.at[PER * j : PER * j + PER]
        remote(part, part, dsend, drecv.at[j], ep, tp).wait_recv()

    first.wait_recv()
    later_core = c == 1
    mine, other = msg[0:128, :], pmsg[0:128, :]
    older = jnp.where(later_core, other, mine)
    newer = jnp.where(later_core, mine, other)
    newer_total = jnp.where(later_core, msg[128:136, :], pmsg[128:136, :])
    joint[...] = column(newer_total) * older + newer
    half = pl.ds(pl.multiple_of(c * 64, 64), 64)
    chmsg[0:64, :] = joint[half, :]
    chmsg[64:72, :] = msg[128:136, :] + pmsg[128:136, :]
    hops = [(dz, dy) for dz in range(NZ) for dy in range(NY) if (dz, dy) != (0, 0)]

    def share(k):
        to = target((*hops[k], 0))
        return to // NC, remote(chmsg, chrecv.at[chip], ch_ssem.at[k], ch_rsem.at[chip], to, tp)

    for k in range(len(hops)):
        to_chip, cp = share(k)
        pl.when(to_chip > chip)(cp.start)
    for s in range(16, 32):
        dispatch(s)

    for i in range(7, 11):
        loads[i].wait()
    arrived(0)
    expert(0)
    arrived(1)
    expert(1)

    inc[half, :] = jnp.zeros((64, 128), F32)

    def join(k, _):
        cp = remote(chrecv.at[k], chrecv.at[k], ch_ssem.at[0], ch_rsem.at[k], ep, tp)
        cp.wait_recv()
        fade = column(chrecv[k, 64:72, :])
        inc[half, :] = jnp.where(later_core, fade[64:128], fade[0:64]) * inc[half, :] + chrecv[k, 0:64, :]
        return 0

    lax.fori_loop(0, chip, join, 0)
    second = remote(inc.at[half], inc.at[half], dd_ssem.at[1], dd_rsem.at[1], partner, tp)
    second.start()
    reduce(0)
    second.wait()
    joined = column(pmsg[128:136, :]) * inc[...] + pmsg[0:128, :]
    entry = jnp.where(later_core, joined, inc[...])
    entry_bd = jnp.concatenate([entry, entry], axis=1) * own_head
    for i in range(att.shape[0] // 128):
        rows = slice(128 * i, 128 * i + 128)
        whole = att[rows, :] + dot(reach[rows, :], entry_bd, HIGH)
        parts = []
        for h in range(2):
            one = whole[:, VALUE_DIM * h : VALUE_DIM * (h + 1)]
            parts.append(one * lax.rsqrt(jnp.mean(one * one, axis=-1, keepdims=True) + EPS))
        out_gate = proj[rows, 512:768]
        gated = jnp.concatenate(parts, axis=1) * hgain_ref[...] * (out_gate * jax.nn.sigmoid(out_gate))
        mpart[rows, :] = dot(gated.astype(BF16), wmix[...]).astype(BF16)
    quarter = out1_ref.shape[0]
    for d in (1, 3, 2):
        t = (tp + d) % 4
        rows = pl.ds(pl.multiple_of(t * quarter, quarter), quarter)
        remote(mpart.at[rows], mrecv.at[d - 1], mx_ssem, mx_rsem, ep, t).start()

    arrived(2)
    expert(2)
    reduce(1)
    arrived(3)
    expert(3)
    reduce(2)
    remote(mrecv, mrecv, mx_ssem, mx_rsem, ep, tp).wait_recv()
    rows = pl.ds(pl.multiple_of(tp * quarter, quarter), quarter)
    whole = mpart[rows, :].astype(F32)
    for d in range(3):
        whole = whole + mrecv[d].astype(F32)
    out1_ref[...] = whole.astype(BF16)
    reduce(3)

    e_lane = iota((rows2, experts), 1)
    r_cols = [routes_ref[:, 0:1], routes_ref[:, 1:2]]
    member = ((r_cols[0] == e_lane) | (r_cols[1] == e_lane)).astype(BF16)
    earlier = (iota((rows2, rows2), 0) > iota((rows2, rows2), 1)).astype(BF16)
    rank = dot(earlier, member)
    spread = iota((rows2, experts * CAP), 1).astype(F32)
    picks = []
    for r in range(2):
        slot = jnp.sum(jnp.where(r_cols[r] == e_lane, rank, 0.0), axis=1, keepdims=True)
        place = slot + (r_cols[r] * CAP).astype(F32)
        picks.append((spread == place).astype(BF16))
    remote(rret.at[1:experts], rret.at[1:experts], rt_ssem, rt_rsem, ep, tp).wait_recv()
    flat = rret[...].reshape(experts * CAP, 512)
    mixed = jnp.zeros((rows2, 512), F32)
    for r in range(2):
        share_r = jax.nn.sigmoid(logits_ref[:, r : r + 1] - logits_ref[:, 1 - r : 2 - r])
        mixed = mixed + dot(picks[r], flat) * share_r
    out2_ref[...] = mixed.astype(BF16)

    remote(send2.at[1:experts], send2.at[1:experts], dsend, drecv.at[0], ep, tp).wait_send()
    for j in range(CHUNKS):
        remote(prs.at[j], prs.at[j], rs_ssem, rs_rsem.at[j], ep, tp).wait_send()
    remote(mrecv, mrecv, mx_ssem, mx_rsem, ep, tp).wait_send()
    remote(rret.at[1:experts], rret.at[1:experts], rt_ssem, rt_rsem, ep, tp).wait_send()
    first.wait_send()
    for k in range(len(hops)):
        to_chip, cp = share(k)
        pl.when(to_chip > chip)(cp.wait_send)


def body(
    tokens_first, norm_gain_first, w_query, w_key, w_value, w_outgate, w_decay, decay_bias,
    head_gain, w_mix_out, tokens_second, norm_gain_second, routes, route_logits,
    expert_gate, expert_up, expert_down,
):
    hbm, vmem = pl.BlockSpec(memory_space=pl.ANY), pl.BlockSpec(memory_space=pltpu.VMEM)
    rows1, width = tokens_first.shape
    rows2 = tokens_second.shape[0]
    hidden = expert_gate.shape[2]
    experts = NZ * NY * NC
    quarter = width // 4
    V, D = pltpu.VMEM, pltpu.SemaphoreType.DMA
    return pl.pallas_call(
        kernel,
        out_shape=(
            jax.ShapeDtypeStruct((rows1 // 4, width), BF16),
            jax.ShapeDtypeStruct((rows2, quarter), BF16),
        ),
        in_specs=[
            hbm, vmem, hbm, hbm, hbm, hbm, hbm, vmem, vmem, hbm,
            hbm, vmem, vmem, vmem, vmem, hbm, hbm, hbm,
        ],
        out_specs=(vmem, vmem),
        scratch_shapes=[
            V((rows2, width), BF16), V((rows2, width), BF16),
            V((experts, CAP, width), BF16), V((experts, CAP, width), BF16),
            V((rows1, width), BF16), V((rows1, width), BF16),
            V((width, 896), BF16), V((256, width), BF16),
            V((width, hidden), BF16), V((width, hidden), BF16), V((hidden, width), BF16),
            V((rows1, 896), F32), V((rows1, 256), F32), V((rows1, 128), F32),
            V((128, 256), F32), V((8, 128), F32), V((136, 128), F32), V((136, 128), F32),
            V((128, 128), F32), V((128, 128), F32),
            V((CHUNKS, 4, PER * CAP, quarter), BF16), V((CHUNKS, 3, PER * CAP, quarter), BF16),
            V((CHUNKS, PER, CAP, quarter), BF16), V((experts, CAP, quarter), BF16),
            V((rows1, width), BF16), V((3, rows1 // 4, width), BF16),
            V((PER * CAP, hidden), BF16), V((72, 128), F32), V((NZ * NY, 72, 128), F32),
            D((11,)), D(()), D((CHUNKS,)), D(()), D((CHUNKS,)), D(()), D(()), D(()), D(()),
            D((2,)), D((2,)), D((15,)), D((16,)),
        ],
        compiler_params=pltpu.CompilerParams(
            collective_id=0, has_side_effects=True, vmem_limit_bytes=63 * 2**20
        ),
        name="layer",
    )(
        tokens_first, norm_gain_first.reshape(1, -1), w_query, w_key, w_value, w_outgate, w_decay,
        decay_bias, head_gain.reshape(1, -1), w_mix_out, tokens_second,
        norm_gain_second.reshape(1, -1), routes, routes.T, route_logits,
        expert_gate, expert_up, expert_down,
    )


def solution(mesh):
    ep_tp = ("ep", "tp")
    in_specs = (
        P("ep", None), P(), P(None, "tp"), P(None, "tp"), P(None, "tp"), P(None, "tp"),
        P(None, "tp"), P("ep", "tp"), P("tp"), P("tp", None), P("ep", None), P(), P("ep", None),
        P("ep", None), P("ep", None, "tp"), P("ep", None, "tp"), P("ep", "tp", None),
    )
    out_specs = (P(ep_tp, None), P("ep", "tp"))
    return jax.shard_map(body, mesh=mesh, in_specs=in_specs, out_specs=out_specs, check_vma=False)
```

time: 227 us -> 114 us (0.50)
  Pallas kernels: 0 us -> 106 us
  local copies, waits for them, and re-layouts: 58.1 us -> 6.5 us
  matrix products: 42.5 us -> 0 us
  other arithmetic: 29.8 us -> 0 us
  waiting for transfers between devices: 27.9 us -> 0 us
  starting transfers between devices: 27.5 us -> 0 us
  blocking collectives: 24.2 us -> 0 us
  between operations: 14.7 us -> 0.64 us
    pallas_call x0 -> x1, Pallas kernels: none -> 106 us  [body(): pl.pallas_call(kernel, out_shape=(jax.ShapeDtypeStruct((rows1 // 4, width...]
    dot_general x42 -> x0, matrix products: 42.5 us -> none  [the longest x8 6.66 us: block_step(): jnp.einsum('azm,zmj->azj', forward_decay_rows, entry_state, precision=lax...]
    all_to_all x4 -> x0, starting transfers between devices: 27.5 us -> none  [the longest x1 9.79 us: body(): lax.all_to_all(buffer, EP, split_axis=0, concat_axis=0, tiled=True)]
    all_to_all x4 -> x0, waiting for transfers between devices: 27.2 us -> none  [the longest x1 13.4 us: summed_on_arrival(): lax.all_to_all(cut_along(shard, dim, devices), axis, 0, 0, tiled=True)]
    all_gather x3 -> x0, blocking collectives: 24.2 us -> none  [all_in_one(): both, at, found = (lax.all_gather(jnp.concatenate(lines), axis), 0, {})]
    reshape x10 -> x0, local copies, waits for them, and re-layouts: 16.3 us -> none  [the longest x1 4.15 us: body(): copy_rows = jnp.repeat(normed_second, route_count, axis=0)]
    dynamic_slice x16 -> x0, local copies, waits for them, and re-layouts: 13.6 us -> none  [body(): lax.scan(block_step, start_state, (query_wide, key_wide, value_wide, log_...]
    reduce_sum x5 -> x0, other arithmetic: 12.1 us -> none  [the longest x1 4.36 us: summed_on_arrival(): return jnp.sum(pieces.astype(jnp.float32), axis=0)]
  transfers between devices with their start and end apart: 5 -> 0, of which waited for: 3 -> 0; matrix products, arithmetic and copies ran while one was open for 53% -> 0% of each run, Pallas kernels for 0% -> 0%
where the time goes in v1:
time: 114 us; the launch traced here: 113 us
  Pallas kernels  106 us (93%)
  local copies, waits for them, and re-layouts  6.5 us (6%)
    pallas_call x1, Pallas kernels, body(): pl.pallas_call(kernel, out_shape=(jax.ShapeDtypeStruct((rows1 // 4, width...  106 us
    unnamed x4, local copies, waits for them, and re-layouts  6.5 us

profile of v1, /device:TPU:1, one launch (start us, length us, event | category | flops | bytes accessed | tf_op | source)
XLA Modules:
  0.0 113.3 jit_solution(7042716509091369333)
XLA Ops:
  0.6 1.5 %copy.20.logits_ref = f32[256,2]{1,0:T(8,128)} copy(f32[256,2]{0,1:T(2,128)} %param.30) | data formatting | bytes 4096 | tf_op args[13]
  2.1 1.5 %copy.19.routes_ref = s32[256,2]{1,0:T(8,128)} copy(s32[256,2]{0,1:T(2,128)} %param.29) | data formatting | bytes 4096 | tf_op args[12]
  3.6 106.2 %layer.1 = (bf16[128,2048]{1,0:T(8,128)(2,1)}, bf16[256,512]{1,0:T(8,128)(2,1)}) custom-call(bf16[512,2048]{1,0:T(8,128)(2,1)} %tok1_h.1, f32[1,2048]{1,0:T(1,128)} %bitcast.4, bf16[2048,128]{1,0:T(8,128)(2,1)} %wq_h.1, bf16[2048,128]{1,0:T(8,128)(2,1)} %wk_h.1, bf16[2048,256]{1,0:T(8,128)(2,1)} %wv_h.1, bf16[2048,256]{1,0:T(8,128)(2,1)} %wo_h.1, ...), custom_call_target="tpu_custom_call" | custom-call | tf_op jit(solution)/shard_map/layer/pallas_call | solution.py:330
  109.7 1.9 %copy.23 = bf16[128,2048]{1,0:T(8,128)(2,1)} copy(bf16[128,2048]{1,0:T(8,128)(2,1)} %get-tuple-element.4) | data formatting | bytes 1048576
  111.6 1.7 %copy.24 = bf16[256,512]{1,0:T(8,128)(2,1)} copy(bf16[256,512]{1,0:T(8,128)(2,1)} %get-tuple-element.5) | data formatting | bytes 524288

commit v2 on v1

v2 whole, which is shorter than its diff:
```python
import jax
import jax.numpy as jnp
from jax import lax
from jax.experimental import pallas as pl
from jax.experimental.pallas import tpu as pltpu
from jax.sharding import PartitionSpec as P

KEY_DIM = 64
VALUE_DIM = 128
BLOCK = 64
CAP = 32
EPS = 1e-06
TEMPER = 16.0
NZ, NY, NC = 4, 4, 2
MESH = pl.DeviceIdType.MESH
HIGH = lax.Precision.HIGHEST
F32, BF16 = jnp.float32, jnp.bfloat16

NEAR, FAR = (1, 3), (2,)
ORDER = (
    [(0, 0, 0), (0, 0, 1)]
    + [o for d in NEAR for o in ((d, 0, 0), (0, d, 0))]
    + [(dz, dy, c) for dz in NEAR for dy in NEAR for c in (0, 1)]
    + [o for c in (0, 1) for o in ((2, 0, c), (0, 2, c))]
    + [o for d in NEAR for o in ((d, 2, 0), (2, d, 1))]
    + [o for d in NEAR for o in ((2, d, 0), (d, 2, 1))]
    + [(2, 2, 0), (2, 2, 1)]
    + [o for d in NEAR for o in ((d, 0, 1), (0, d, 1))]
)
SLOT = {o: s for s, o in enumerate(ORDER)}
SIZES = (6, 8, 8, 6, 4)
START = [sum(SIZES[:j]) for j in range(len(SIZES))]
CHUNKS = len(SIZES)


def dot(a, b, precision=None):
    return jnp.dot(a, b, preferred_element_type=F32, precision=precision)


def dot_t0(a, b, precision=None):
    return lax.dot_general(
        a, b, (((0,), (0,)), ((), ())), preferred_element_type=F32, precision=precision
    )


def dot_t1(a, b, precision=None):
    return lax.dot_general(
        a, b, (((1,), (1,)), ((), ())), preferred_element_type=F32, precision=precision
    )


def iota(shape, dim):
    return lax.broadcasted_iota(jnp.int32, shape, dim)


def rms(rows, gain):
    wide = rows.astype(F32)
    return wide * lax.rsqrt(jnp.mean(wide * wide, axis=-1, keepdims=True) + EPS) * gain


def log_sigmoid(x):
    return jnp.minimum(x, 0.0) - jnp.log1p(jnp.exp(-jnp.abs(x)))


def kernel(
    tok1_h, g1_ref, wq_h, wk_h, wv_h, wo_h, wd_h, bias_ref, hgain_ref, wmix_h,
    tok2_h, g2_ref, routes_t_ref, logits_t_ref, wg_h, wu_h, wdn_h,
    out1_ref, out2_ref,
    tok2, norm2, send2, recv2, relay, tok1, norm1, w1, wfull, wg, wu, wdn, proj, att, reach,
    sbd, total, msg, pmsg, inc, joint, psend, r1, s2, r2, rsend, rret, gated, spread, pickm, hid,
    chmsg, ymsg, zmsg, yrecv, zrecv,
    ld, dsend, drecv, hand_sem, rs_ssem, r1_rsem, r2_rsem, w_ssem, w_rsem, mx_ssem, mx_rsem, rt_ssem, rt_rsem,
    dd_ssem, dd_rsem, ch_ssem, y_rsem, zm_ssem, z_rsem,
):
    ep, tp = lax.axis_index("ep"), lax.axis_index("tp")
    z, y, c = ep // (NY * NC), (ep // NC) % NY, ep % NC
    chip = z * NY + y
    flips = (tp, tp + 1 - 2 * (tp % 2), (tp + 2) % 4, 3 - tp)
    partner = ep + 1 - 2 * c

    def target(o, sign=1):
        dz, dy, dc = o
        return (
            ((z + sign * dz + NZ) % NZ) * (NY * NC)
            + ((y + sign * dy + NY) % NY) * NC
            + (c + dc) % NC
        )

    def remote(src, dst, ssem, rsem, to_ep, to_tp):
        return pltpu.make_async_remote_copy(
            src_ref=src, dst_ref=dst, send_sem=ssem, recv_sem=rsem,
            device_id=(to_ep, to_tp), device_id_type=MESH,
        )

    loads = [
        (tok2_h, tok2), (tok1_h, tok1),
        (wq_h, w1.at[:, 0:128]), (wk_h, w1.at[:, 128:256]), (wv_h, w1.at[:, 256:512]),
        (wo_h, w1.at[:, 512:768]), (wd_h, w1.at[:, 768:896]),
        (wg_h.at[0], wg), (wu_h.at[0], wu), (wdn_h.at[0], wdn),
        (wmix_h, wfull.at[pl.ds(pl.multiple_of(tp * 256, 256), 256)]),
    ]
    loads = [pltpu.make_async_copy(s, d, ld.at[i]) for i, (s, d) in enumerate(loads)]
    for cp in loads:
        cp.start()

    barrier = pltpu.get_barrier_semaphore()
    for o in ORDER[1:]:
        pl.semaphore_signal(barrier, inc=1, device_id=(target(o), tp), device_id_type=MESH)
    for d in range(1, 4):
        pl.semaphore_signal(barrier, inc=1, device_id=(ep, (tp + d) % 4), device_id_type=MESH)

    rows2 = norm2.shape[0]
    experts = send2.shape[0]
    r0t, r1t = routes_t_ref[0:1, :], routes_t_ref[1:2, :]
    e_sub = iota((experts, rows2), 0)
    gap = logits_t_ref[0:1, :] - logits_t_ref[1:2, :]
    share_t = jnp.concatenate([jax.nn.sigmoid(gap), jax.nn.sigmoid(-gap)], axis=0)
    member_t = ((r0t == e_sub) | (r1t == e_sub)).astype(F32)
    before_t = (iota((rows2, rows2), 0) < iota((rows2, rows2), 1)).astype(BF16)
    rank_t = dot(member_t.astype(BF16), before_t)
    place_t = jnp.where(member_t > 0.0, rank_t, -1.0)
    loads[0].wait()
    norm2[...] = rms(tok2[...], g2_ref[...]).astype(BF16)
    for g in range(experts // 8):
        place = place_t[8 * g : 8 * g + 8]
        want = iota((8, CAP, rows2), 1).astype(F32)
        pick = (place[:, None, :] == want).astype(BF16).reshape(8 * CAP, rows2)
        for n in range(norm2.shape[1] // 512):
            cols = slice(512 * n, 512 * n + 512)
            send2[8 * g : 8 * g + 8, :, cols] = (
                dot(pick, norm2[:, cols]).astype(BF16).reshape(8, CAP, 512)
            )
    pl.semaphore_wait(barrier, len(ORDER) - 1 + 3)

    def straight(o):
        to, s = target(o), SLOT[o]
        remote(send2.at[to], recv2.at[s], dsend, drecv.at[s], to, tp).start()

    def turn(o):
        dz, dy, dc = o
        corner = target((0, dy, 1) if dc else (dz, 0, 0))
        onward = target((dz, 0, 0) if dc else (0, dy, 0))
        k = (dc * 3 + dz - 1) * 3 + dy - 1
        into = remote(send2.at[target(o)], relay.at[k], dsend, hand_sem.at[k], corner, tp)
        s = SLOT[o]
        out = remote(relay.at[k], recv2.at[s], dsend, drecv.at[s], onward, tp)
        return into, out

    def leave(dzs, dys):
        for dz in dzs:
            for dy in dys:
                turn((dz, dy, 0))[0].start()
                turn((dy, dz, 1))[0].start()

    def pass_on(dzs, dys):
        for dz in dzs:
            for dy in dys:
                for o in ((dz, dy, 0), (dy, dz, 1)):
                    into, out = turn(o)
                    into.wait_recv()
                    out.start()

    leave(NEAR, NEAR)
    straight((0, 0, 1))
    for d in NEAR:
        straight((d, 0, 0))
        straight((0, d, 0))
    leave(NEAR, FAR)
    leave(FAR, NEAR)
    leave(FAR, FAR)

    def shard_rows(t, core, lo, n):
        start = t * 256 + core * 128 + lo
        return pl.ds(pl.multiple_of(start, 64), n)

    def hand_on(owner, lo, n, k, to_ep, to_tp):
        rows = shard_rows(owner, c, lo, n)
        remote(wfull.at[rows], wfull.at[rows], w_ssem, w_rsem.at[k], to_ep, to_tp).start()

    def handed(n, k):
        remote(wfull.at[0:n], wfull.at[0:n], w_ssem, w_rsem.at[k], ep, tp).wait_recv()

    loads[10].wait()
    hand_on(tp, 0, 64, 0, ep, flips[1])
    hand_on(tp, 64, 64, 1, ep, flips[3])
    recv2[0] = send2[ep]

    loads[1].wait()
    for i in range(tok1.shape[0] // 128):
        rows = slice(128 * i, 128 * i + 128)
        norm1[rows, :] = rms(tok1[rows, :], g1_ref[...]).astype(BF16)
    for i in range(2, 7):
        loads[i].wait()
    for lo, hi in ((0, 256), (256, 512), (512, 768), (768, 896)):
        proj[:, lo:hi] = dot(norm1[...], w1[:, lo:hi])
    sbd[...] = jnp.zeros_like(sbd)
    total[...] = jnp.zeros_like(total)
    own_head = (iota(sbd.shape, 0) // KEY_DIM == iota(sbd.shape, 1) // VALUE_DIM).astype(F32)
    tri = (iota((BLOCK, BLOCK), 0) >= iota((BLOCK, BLOCK), 1)).astype(F32)
    head_lane = iota((BLOCK, 2 * KEY_DIM), 1) // KEY_DIM

    def block(b, _):
        rows = pl.ds(pl.multiple_of(b * BLOCK, BLOCK), BLOCK)
        query = (proj[rows, 0:128] * KEY_DIM ** (-0.5)).astype(BF16).astype(F32)
        key = proj[rows, 128:256].astype(BF16).astype(F32)
        value = proj[rows, 256:512].astype(BF16).astype(F32)
        log_decay = log_sigmoid(proj[rows, 768:896] + bias_ref[pl.ds(b, 1), :]) / TEMPER
        cumul = dot(tri, log_decay, HIGH)
        final = cumul[BLOCK - 1 : BLOCK, :]
        forward = query * jnp.exp(cumul)
        behind = key * jnp.exp(-cumul)
        fading = key * jnp.exp(final - cumul)
        within = []
        for h in range(2):
            mine = jnp.where(head_lane == h, forward, 0.0)
            scores = dot_t1(mine, behind, HIGH)
            scores = jnp.where(tri > 0.0, scores, 0.0)
            within.append(dot(scores, value[:, VALUE_DIM * h : VALUE_DIM * (h + 1)], HIGH))
        att[rows, :] = jnp.concatenate(within, axis=1) + dot(forward, sbd[...], HIGH)
        fall = dot_t0(log_decay, jnp.ones((BLOCK, sbd.shape[1]), F32), HIGH)
        sbd[...] = jnp.exp(fall) * sbd[...] + own_head * dot_t0(fading, value, HIGH)
        reach[rows, :] = query * jnp.exp(cumul + total[0:1, :])
        total[0:1, :] = total[0:1, :] + final
        return 0

    blocks = proj.shape[0] // BLOCK
    lax.fori_loop(0, blocks // 2, block, 0)
    handed(64, 0)
    hand_on(tp, 0, 64, 2, ep, flips[3])
    hand_on(flips[1], 0, 64, 2, ep, flips[3])
    handed(64, 1)
    hand_on(tp, 64, 64, 3, ep, flips[1])
    hand_on(flips[3], 64, 64, 3, ep, flips[1])
    pass_on(NEAR, NEAR)
    lax.fori_loop(blocks // 2, blocks, block, 0)
    msg[0:64, :] = sbd[0:64, 0:128]
    msg[64:128, :] = sbd[64:128, 128:256]
    msg[128:136, :] = total[...]
    first = remote(msg, pmsg, dd_ssem.at[0], dd_rsem.at[0], partner, tp)
    first.start()

    def column(row8):
        return jnp.exp(dot_t0(row8, jnp.ones((8, 128), F32), HIGH))

    def rows_of(j, p=None):
        lo, n = START[j] * CAP, SIZES[j] * CAP
        return slice(lo, lo + n) if p is None else slice(lo + p * n // 2, lo + (p + 1) * n // 2)

    def expert(j):
        n = SIZES[j]
        x_rows = recv2[START[j] : START[j] + n].reshape(n * CAP, recv2.shape[2])
        for lo in range(0, hid.shape[1], 256):
            cols = slice(lo, lo + 256)
            gate = dot(x_rows, wg[:, cols])
            up = dot(x_rows, wu[:, cols])
            hid[0 : n * CAP, cols] = (gate * jax.nn.sigmoid(gate) * up).astype(BF16)
        for m in (2, 1, 3, 0):
            cols = pl.ds(pl.multiple_of(flips[m] * 512, 512), 512)
            psend[m, rows_of(j), :] = dot(hid[0 : n * CAP, :], wdn[:, cols]).astype(BF16)
            for p, q, k in ((0, 1, 0), (0, 2, 1), (1, 3, 0), (1, 2, 1)):
                if q == m:
                    remote(
                        psend.at[m, rows_of(j, p)], r1.at[k, rows_of(j, p)],
                        rs_ssem, r1_rsem.at[j, p], ep, flips[1 + 2 * p],
                    ).start()

    def middle(j):
        for p in range(2):
            rows = rows_of(j, p)
            both = r1.at[:, rows]
            remote(both, both, rs_ssem, r1_rsem.at[j, p], ep, tp).wait_recv()
            pair = psend[3 - 2 * p, rows, :].astype(F32) + r1[1, rows, :].astype(F32)
            s2[rows, :] = pair.astype(BF16)
            remote(s2.at[rows], r2.at[rows], rs_ssem, r2_rsem.at[j, p], ep, flips[3 - 2 * p]).start()

    def reduce(j):
        for p in range(2):
            rows = rows_of(j, p)
            remote(r2.at[rows], r2.at[rows], rs_ssem, r2_rsem.at[j, p], ep, tp).wait_recv()
            whole = psend[0, rows, :].astype(F32) + r1[0, rows, :].astype(F32) + r2[rows, :].astype(F32)
            first_slot, n = START[j] + p * SIZES[j] // 2, SIZES[j] // 2
            rsend[first_slot : first_slot + n] = whole.astype(BF16).reshape(n, CAP, 512)
            for s in range(first_slot, first_slot + n):
                if s == 0:
                    rret[ep] = rsend[0]
                else:
                    to = target(ORDER[s], -1)
                    remote(rsend.at[s], rret.at[ep], rt_ssem, rt_rsem, to, tp).start()

    def arrived(j):
        for s in range(max(START[j], 1), START[j] + SIZES[j]):
            remote(recv2.at[s], recv2.at[s], dsend, drecv.at[s], ep, tp).wait_recv()

    first.wait_recv()
    later_core = c == 1
    mine, other = msg[0:128, :], pmsg[0:128, :]
    older = jnp.where(later_core, other, mine)
    newer = jnp.where(later_core, mine, other)
    newer_total = jnp.where(later_core, msg[128:136, :], pmsg[128:136, :])
    joint[...] = column(newer_total) * older + newer
    half = pl.ds(pl.multiple_of(c * 64, 64), 64)
    chmsg[0:64, :] = joint[half, :]
    chmsg[64:72, :] = msg[128:136, :] + pmsg[128:136, :]
    yrecv[y] = chmsg[...]

    def y_share(d):
        return remote(chmsg, yrecv.at[y], ch_ssem, y_rsem.at[d - 1], target((0, d, 0)), tp)

    def z_share(d):
        return remote(zmsg, zrecv.at[d - 1], zm_ssem.at[d - 1], z_rsem.at[d - 1], target((d, 0, 0)), tp)

    for d in range(1, NY):
        y_share(d).start()
    for dc in (0, 1):
        straight((2, 0, dc))
        straight((0, 2, dc))

    for i in range(7, 10):
        loads[i].wait()
    arrived(0)
    expert(0)
    pass_on(NEAR, FAR)
    handed(128, 2)
    handed(128, 3)
    for m in range(1, 4):
        hand_on(flips[m], 0, 128, 4, partner, tp)
    middle(0)
    pass_on(FAR, NEAR)
    pass_on(FAR, FAR)
    for d in NEAR:
        straight((d, 0, 1))
        straight((0, d, 1))
    cols_in = jnp.concatenate(
        [routes_t_ref[...].astype(F32), share_t, jnp.zeros((4, rows2), F32)], axis=0
    )
    unit = (iota((8, 128), 0) == iota((8, 128), 1)).astype(F32)
    cols_out = dot_t0(cols_in, unit, HIGH)
    e_lane = iota((rows2, experts), 1).astype(F32)
    r_cols = [cols_out[:, 0:1], cols_out[:, 1:2]]
    member = ((r_cols[0] == e_lane) | (r_cols[1] == e_lane)).astype(BF16)
    earlier = (iota((rows2, rows2), 0) > iota((rows2, rows2), 1)).astype(BF16)
    rank = dot(earlier, member)
    lanes = iota((rows2, experts * CAP), 1).astype(F32)
    for r in range(2):
        slot = jnp.sum(jnp.where(r_cols[r] == e_lane, rank, 0.0), axis=1, keepdims=True)
        pickm[r] = (lanes == slot + r_cols[r] * CAP).astype(BF16)

    arrived(1)
    expert(1)
    reduce(0)

    def fade_of(row8):
        fade = column(row8)
        return jnp.where(later_core, fade[64:128], fade[0:64])

    for d in range(1, NY):
        y_share(d).wait_recv()
    row_state, row_total = yrecv[0, 0:64, :], yrecv[0, 64:72, :]
    own_state = jnp.zeros_like(row_state)
    own_total = jnp.zeros_like(row_total)
    for k in range(1, NY):
        own_state = jnp.where(y == k, row_state, own_state)
        own_total = jnp.where(y == k, row_total, own_total)
        row_state = fade_of(yrecv[k, 64:72, :]) * row_state + yrecv[k, 0:64, :]
        row_total = row_total + yrecv[k, 64:72, :]
    ymsg[0:64, :], ymsg[64:72, :] = own_state, own_total
    zmsg[0:64, :], zmsg[64:72, :] = row_state, row_total
    for d in range(1, NZ):
        pl.when(z + d < NZ)(z_share(d).start)
    middle(1)
    arrived(2)
    expert(2)
    reduce(1)
    inc[half, :] = jnp.zeros((64, 128), F32)

    def join(k, _):
        cp = remote(zrecv.at[z - k - 1], zrecv.at[z - k - 1], ch_ssem, z_rsem.at[z - k - 1], ep, tp)
        cp.wait_recv()
        fade = fade_of(zrecv[z - k - 1, 64:72, :])
        inc[half, :] = fade * inc[half, :] + zrecv[z - k - 1, 0:64, :]
        return 0

    lax.fori_loop(0, z, join, 0)
    inc[half, :] = fade_of(ymsg[64:72, :]) * inc[half, :] + ymsg[0:64, :]
    second = remote(inc.at[half], inc.at[half], dd_ssem.at[1], dd_rsem.at[1], partner, tp)
    second.start()
    arrived(3)
    expert(3)
    second.wait()
    joined = column(pmsg[128:136, :]) * inc[...] + pmsg[0:128, :]
    entry = jnp.where(later_core, joined, inc[...])
    entry_bd = jnp.concatenate([entry, entry], axis=1) * own_head
    for i in range(att.shape[0] // 128):
        rows = slice(128 * i, 128 * i + 128)
        whole = att[rows, :] + dot(reach[rows, :], entry_bd, HIGH)
        parts = []
        for h in range(2):
            one = whole[:, VALUE_DIM * h : VALUE_DIM * (h + 1)]
            parts.append(one * lax.rsqrt(jnp.mean(one * one, axis=-1, keepdims=True) + EPS))
        out_gate = proj[rows, 512:768]
        rows_out = jnp.concatenate(parts, axis=1) * hgain_ref[...]
        gated[rows, :] = (rows_out * (out_gate * jax.nn.sigmoid(out_gate))).astype(BF16)
    quarter = out1_ref.shape[0]
    mine_cols = pl.ds(pl.multiple_of(tp * 256, 256), 256)
    for m in range(1, 4):
        rows = pl.ds(pl.multiple_of(flips[m] * quarter, quarter), quarter)
        remote(gated.at[rows], spread.at[:, mine_cols], mx_ssem, mx_rsem, ep, flips[m]).start()
    spread[:, mine_cols] = gated[pl.ds(pl.multiple_of(tp * quarter, quarter), quarter), :]

    middle(2)
    arrived(4)
    expert(4)
    reduce(2)
    remote(spread.at[:, 0:768], spread.at[:, 0:768], mx_ssem, mx_rsem, ep, tp).wait_recv()
    handed(384, 4)
    for n in range(4):
        cols = slice(512 * n, 512 * n + 512)
        out1_ref[:, cols] = dot(spread[...], wfull[:, cols]).astype(BF16)
    middle(3)
    middle(4)
    reduce(3)
    reduce(4)

    remote(rret.at[1:experts], rret.at[1:experts], rt_ssem, rt_rsem, ep, tp).wait_recv()
    flat = rret[...].reshape(experts * CAP, 512)
    mixed = jnp.zeros((rows2, 512), F32)
    for r in range(2):
        mixed = mixed + dot(pickm[r], flat) * cols_out[:, 2 + r : 3 + r]
    out2_ref[...] = mixed.astype(BF16)

    remote(send2.at[1:experts], send2.at[1:experts], dsend, drecv.at[0], ep, tp).wait_send()
    remote(relay, relay, dsend, drecv.at[0], ep, tp).wait_send()
    remote(r1, r1, rs_ssem, r1_rsem.at[0, 0], ep, tp).wait_send()
    remote(r2, r2, rs_ssem, r1_rsem.at[0, 0], ep, tp).wait_send()
    for n in (128, 256, 384):
        remote(wfull.at[0:n], wfull.at[0:n], w_ssem, w_rsem.at[0], ep, tp).wait_send()
    remote(spread.at[:, 0:768], spread.at[:, 0:768], mx_ssem, mx_rsem, ep, tp).wait_send()
    remote(rret.at[1:experts], rret.at[1:experts], rt_ssem, rt_rsem, ep, tp).wait_send()
    first.wait_send()
    remote(yrecv.at[0:3], yrecv.at[0:3], ch_ssem, y_rsem.at[0], ep, tp).wait_send()
    for d in range(1, NZ):
        pl.when(z + d < NZ)(z_share(d).wait_send)


def body(
    tokens_first, norm_gain_first, w_query, w_key, w_value, w_outgate, w_decay, decay_bias,
    head_gain, w_mix_out, tokens_second, norm_gain_second, routes, route_logits,
    expert_gate, expert_up, expert_down,
):
    hbm, vmem = pl.BlockSpec(memory_space=pl.ANY), pl.BlockSpec(memory_space=pltpu.VMEM)
    rows1, width = tokens_first.shape
    rows2 = tokens_second.shape[0]
    hidden = expert_gate.shape[2]
    experts = NZ * NY * NC
    quarter = width // 4
    V, D = pltpu.VMEM, pltpu.SemaphoreType.DMA
    return pl.pallas_call(
        kernel,
        out_shape=(
            jax.ShapeDtypeStruct((rows1 // 4, width), BF16),
            jax.ShapeDtypeStruct((rows2, quarter), BF16),
        ),
        in_specs=[
            hbm, vmem, hbm, hbm, hbm, hbm, hbm, vmem, vmem, hbm,
            hbm, vmem, vmem, vmem, hbm, hbm, hbm,
        ],
        out_specs=(vmem, vmem),
        scratch_shapes=[
            V((rows2, width), BF16), V((rows2, width), BF16),
            V((experts, CAP, width), BF16), V((experts, CAP, width), BF16),
            V((18, CAP, width), BF16),
            V((rows1, width), BF16), V((rows1, width), BF16),
            V((width, 896), BF16), V((1024, width), BF16),
            V((width, hidden), BF16), V((width, hidden), BF16), V((hidden, width), BF16),
            V((rows1, 896), F32), V((rows1, 256), F32), V((rows1, 128), F32),
            V((128, 256), F32), V((8, 128), F32), V((136, 128), F32), V((136, 128), F32),
            V((128, 128), F32), V((128, 128), F32),
            V((4, experts * CAP, quarter), BF16), V((2, experts * CAP, quarter), BF16),
            V((experts * CAP, quarter), BF16), V((experts * CAP, quarter), BF16),
            V((experts, CAP, quarter), BF16), V((experts, CAP, quarter), BF16),
            V((rows1, 256), BF16), V((rows1 // 4, 1024), BF16),
            V((2, rows2, experts * CAP), BF16),
            V((max(SIZES) * CAP, hidden), BF16), V((72, 128), F32), V((72, 128), F32),
            V((72, 128), F32), V((NY, 72, 128), F32), V((NZ - 1, 72, 128), F32),
            D((11,)), D(()), D((32,)), D((18,)), D(()), D((CHUNKS, 2)), D((CHUNKS, 2)), D(()), D((5,)),
            D(()), D(()), D(()), D(()),
            D((2,)), D((2,)), D(()), D((3,)), D((3,)), D((3,)),
        ],
        compiler_params=pltpu.CompilerParams(
            collective_id=0, has_side_effects=True, vmem_limit_bytes=63 * 2**20
        ),
        name="layer",
    )(
        tokens_first, norm_gain_first.reshape(1, -1), w_query, w_key, w_value, w_outgate, w_decay,
        decay_bias, head_gain.reshape(1, -1), w_mix_out, tokens_second,
        norm_gain_second.reshape(1, -1), routes.T, route_logits.T,
        expert_gate, expert_up, expert_down,
    )


def solution(mesh):
    ep_tp = ("ep", "tp")
    in_specs = (
        P("ep", None), P(), P(None, "tp"), P(None, "tp"), P(None, "tp"), P(None, "tp"),
        P(None, "tp"), P("ep", "tp"), P("tp"), P("tp", None), P("ep", None), P(), P("ep", None),
        P("ep", None), P("ep", None, "tp"), P("ep", None, "tp"), P("ep", "tp", None),
    )
    out_specs = (P(ep_tp, None), P("ep", "tp"))
    return jax.shard_map(body, mesh=mesh, in_specs=in_specs, out_specs=out_specs, check_vma=False)
```

time: 114 us -> 95 us (0.83)
  Pallas kernels: 106 us -> 90.6 us
  local copies, waits for them, and re-layouts: 6.5 us -> 3.55 us
    pallas_call x1, Pallas kernels: 106 us -> 90.6 us  [body(): pl.pallas_call(kernel, out_shape=(jax.ShapeDtypeStruct((rows1 // 4, width...]
    unnamed x4 -> x2, local copies, waits for them, and re-layouts: 6.5 us -> 3.55 us
where the time goes in v2:
time: 95 us; the launch traced here: 94.8 us
  Pallas kernels  90.6 us (95%)
  local copies, waits for them, and re-layouts  3.55 us (4%)
    pallas_call x1, Pallas kernels, body(): pl.pallas_call(kernel, out_shape=(jax.ShapeDtypeStruct((rows1 // 4, width...  90.6 us
    unnamed x2, local copies, waits for them, and re-layouts  3.55 us

profile of v2, /device:TPU:1, one launch (start us, length us, event | category | flops | bytes accessed | tf_op | source)
XLA Modules:
  0.0 94.8 jit_solution(12887881470978517994)
XLA Ops:
  0.6 90.6 %layer.1 = (bf16[128,2048]{1,0:T(8,128)(2,1)}, bf16[256,512]{1,0:T(8,128)(2,1)}) custom-call(bf16[512,2048]{1,0:T(8,128)(2,1)} %tok1_h.1, f32[1,2048]{1,0:T(1,128)} %bitcast.5, bf16[2048,128]{1,0:T(8,128)(2,1)} %wq_h.1, bf16[2048,128]{1,0:T(8,128)(2,1)} %wk_h.1, bf16[2048,256]{1,0:T(8,128)(2,1)} %wv_h.1, bf16[2048,256]{1,0:T(8,128)(2,1)} %wo_h.1, ...), custom_call_target="tpu_custom_call" | custom-call | tf_op jit(solution)/shard_map/layer/pallas_call | solution.py:457
  91.2 1.9 %copy.21 = bf16[128,2048]{1,0:T(8,128)(2,1)} copy(bf16[128,2048]{1,0:T(8,128)(2,1)} %get-tuple-element.4) | data formatting | bytes 1048576
  93.1 1.7 %copy.22 = bf16[256,512]{1,0:T(8,128)(2,1)} copy(bf16[256,512]{1,0:T(8,128)(2,1)} %get-tuple-element.5) | data formatting | bytes 524288

commit v3 on v2

--- a/solution.py
+++ b/solution.py
@@ -20,15 +20,15 @@
 ORDER = (
     [(0, 0, 0), (0, 0, 1)]
     + [o for d in NEAR for o in ((d, 0, 0), (0, d, 0))]
-    + [(dz, dy, c) for dz in NEAR for dy in NEAR for c in (0, 1)]
     + [o for c in (0, 1) for o in ((2, 0, c), (0, 2, c))]
+    + [o for d in NEAR for o in ((d, 0, 1), (0, d, 1))]
+    + [(2, 2, 0), (2, 2, 1)]
+    + [o for d in NEAR for o in ((2, d, 0), (d, 2, 1))]
     + [o for d in NEAR for o in ((d, 2, 0), (2, d, 1))]
-    + [o for d in NEAR for o in ((2, d, 0), (d, 2, 1))]
-    + [(2, 2, 0), (2, 2, 1)]
-    + [o for d in NEAR for o in ((d, 0, 1), (0, d, 1))]
+    + [(dz, dy, c) for c in (0, 1) for dz in NEAR for dy in NEAR]
 )
 SLOT = {o: s for s, o in enumerate(ORDER)}
-SIZES = (6, 8, 8, 6, 4)
+SIZES = (6, 8, 6, 4, 4, 4)
 START = [sum(SIZES[:j]) for j in range(len(SIZES))]
 CHUNKS = len(SIZES)
 
@@ -100,14 +100,16 @@
         (wmix_h, wfull.at[pl.ds(pl.multiple_of(tp * 256, 256), 256)]),
     ]
     loads = [pltpu.make_async_copy(s, d, ld.at[i]) for i, (s, d) in enumerate(loads)]
+
+    barrier = pltpu.get_barrier_semaphore()
+    near = [o for o in ORDER[1:] if not (o[0] and o[1])]
+    for o in near:
+        pl.semaphore_signal(barrier, inc=1, device_id=(target(o), tp), device_id_type=MESH)
+    for m in (1, 3):
+        pl.semaphore_signal(barrier, inc=1, device_id=(ep, flips[m]), device_id_type=MESH)
+
     for cp in loads:
         cp.start()
-
-    barrier = pltpu.get_barrier_semaphore()
-    for o in ORDER[1:]:
-        pl.semaphore_signal(barrier, inc=1, device_id=(target(o), tp), device_id_type=MESH)
-    for d in range(1, 4):
-        pl.semaphore_signal(barrier, inc=1, device_id=(ep, (tp + d) % 4), device_id_type=MESH)
 
     rows2 = norm2.shape[0]
     experts = send2.shape[0]
@@ -130,7 +132,7 @@
             send2[8 * g : 8 * g + 8, :, cols] = (
                 dot(pick, norm2[:, cols]).astype(BF16).reshape(8, CAP, 512)
             )
-    pl.semaphore_wait(barrier, len(ORDER) - 1 + 3)
+    pl.semaphore_wait(barrier, len(near) + 2)
 
     def straight(o):
         to, s = target(o), SLOT[o]
@@ -160,14 +162,16 @@
                     into.wait_recv()
                     out.start()
 
-    leave(NEAR, NEAR)
     straight((0, 0, 1))
     for d in NEAR:
         straight((d, 0, 0))
         straight((0, d, 0))
+    leave(FAR, FAR)
+    leave(FAR, NEAR)
+    for dc in (0, 1):
+        straight((2, 0, dc))
+        straight((0, 2, dc))
     leave(NEAR, FAR)
-    leave(FAR, NEAR)
-    leave(FAR, FAR)
 
     def shard_rows(t, core, lo, n):
         start = t * 256 + core * 128 + lo
@@ -231,7 +235,6 @@
     handed(64, 1)
     hand_on(tp, 64, 64, 3, ep, flips[1])
     hand_on(flips[3], 64, 64, 3, ep, flips[1])
-    pass_on(NEAR, NEAR)
     lax.fori_loop(blocks // 2, blocks, block, 0)
     msg[0:64, :] = sbd[0:64, 0:128]
     msg[64:128, :] = sbd[64:128, 128:256]
@@ -311,25 +314,44 @@
 
     for d in range(1, NY):
         y_share(d).start()
-    for dc in (0, 1):
-        straight((2, 0, dc))
-        straight((0, 2, dc))
-
+
+    for d in NEAR:
+        straight((d, 0, 1))
+        straight((0, d, 1))
+    leave(NEAR, NEAR)
     for i in range(7, 10):
         loads[i].wait()
     arrived(0)
     expert(0)
+    pass_on(FAR, FAR)
+    pass_on(FAR, NEAR)
     pass_on(NEAR, FAR)
     handed(128, 2)
     handed(128, 3)
     for m in range(1, 4):
         hand_on(flips[m], 0, 128, 4, partner, tp)
+    arrived(1)
+    expert(1)
     middle(0)
-    pass_on(FAR, NEAR)
-    pass_on(FAR, FAR)
-    for d in NEAR:
-        straight((d, 0, 1))
-        straight((0, d, 1))
+    def fade_of(row8):
+        fade = column(row8)
+        return jnp.where(later_core, fade[64:128], fade[0:64])
+
+    for d in range(1, NY):
+        y_share(d).wait_recv()
+    row_state, row_total = yrecv[0, 0:64, :], yrecv[0, 64:72, :]
+    own_state = jnp.zeros_like(row_state)
+    own_total = jnp.zeros_like(row_total)
+    for k in range(1, NY):
+        own_state = jnp.where(y == k, row_state, own_state)
+        own_total = jnp.where(y == k, row_total, own_total)
+        row_state = fade_of(yrecv[k, 64:72, :]) * row_state + yrecv[k, 0:64, :]
+        row_total = row_total + yrecv[k, 64:72, :]
+    ymsg[0:64, :], ymsg[64:72, :] = own_state, own_total
+    zmsg[0:64, :], zmsg[64:72, :] = row_state, row_total
+    for d in range(1, NZ):
+        pl.when(z + d < NZ)(z_share(d).start)
+    pass_on(NEAR, NEAR)
     cols_in = jnp.concatenate(
         [routes_t_ref[...].astype(F32), share_t, jnp.zeros((4, rows2), F32)], axis=0
     )
@@ -345,32 +367,13 @@
         slot = jnp.sum(jnp.where(r_cols[r] == e_lane, rank, 0.0), axis=1, keepdims=True)
         pickm[r] = (lanes == slot + r_cols[r] * CAP).astype(BF16)
 
-    arrived(1)
-    expert(1)
     reduce(0)
-
-    def fade_of(row8):
-        fade = column(row8)
-        return jnp.where(later_core, fade[64:128], fade[0:64])
-
-    for d in range(1, NY):
-        y_share(d).wait_recv()
-    row_state, row_total = yrecv[0, 0:64, :], yrecv[0, 64:72, :]
-    own_state = jnp.zeros_like(row_state)
-    own_total = jnp.zeros_like(row_total)
-    for k in range(1, NY):
-        own_state = jnp.where(y == k, row_state, own_state)
-        own_total = jnp.where(y == k, row_total, own_total)
-        row_state = fade_of(yrecv[k, 64:72, :]) * row_state + yrecv[k, 0:64, :]
-        row_total = row_total + yrecv[k, 64:72, :]
-    ymsg[0:64, :], ymsg[64:72, :] = own_state, own_total
-    zmsg[0:64, :], zmsg[64:72, :] = row_state, row_total
-    for d in range(1, NZ):
-        pl.when(z + d < NZ)(z_share(d).start)
     middle(1)
     arrived(2)
     expert(2)
     reduce(1)
+    arrived(3)
+    expert(3)
     inc[half, :] = jnp.zeros((64, 128), F32)
 
     def join(k, _):
@@ -384,8 +387,9 @@
     inc[half, :] = fade_of(ymsg[64:72, :]) * inc[half, :] + ymsg[0:64, :]
     second = remote(inc.at[half], inc.at[half], dd_ssem.at[1], dd_rsem.at[1], partner, tp)
     second.start()
-    arrived(3)
-    expert(3)
+    middle(2)
+    arrived(4)
+    expert(4)
     second.wait()
     joined = column(pmsg[128:136, :]) * inc[...] + pmsg[0:128, :]
     entry = jnp.where(later_core, joined, inc[...])
@@ -407,19 +411,20 @@
         remote(gated.at[rows], spread.at[:, mine_cols], mx_ssem, mx_rsem, ep, flips[m]).start()
     spread[:, mine_cols] = gated[pl.ds(pl.multiple_of(tp * quarter, quarter), quarter), :]
 
-    middle(2)
-    arrived(4)
-    expert(4)
+    arrived(5)
+    expert(5)
+    middle(3)
     reduce(2)
+    middle(4)
+    middle(5)
+    reduce(3)
     remote(spread.at[:, 0:768], spread.at[:, 0:768], mx_ssem, mx_rsem, ep, tp).wait_recv()
     handed(384, 4)
     for n in range(4):
         cols = slice(512 * n, 512 * n + 512)
         out1_ref[:, cols] = dot(spread[...], wfull[:, cols]).astype(BF16)
-    middle(3)
-    middle(4)
-    reduce(3)
     reduce(4)
+    reduce(5)
 
     remote(rret.at[1:experts], rret.at[1:experts], rt_ssem, rt_rsem, ep, tp).wait_recv()
     flat = rret[...].reshape(experts * CAP, 512)

time: 95 us -> 88.2 us (0.928)
  Pallas kernels: 90.6 us -> 83.8 us
    pallas_call x1, Pallas kernels: 90.6 us -> 83.8 us  [body(): pl.pallas_call(kernel, out_shape=(jax.ShapeDtypeStruct((rows1 // 4, width...]
where the time goes in v3:
time: 88.2 us; the launch traced here: 88 us
  Pallas kernels  83.8 us (95%)
  local copies, waits for them, and re-layouts  3.55 us (4%)
    pallas_call x1, Pallas kernels, body(): pl.pallas_call(kernel, out_shape=(jax.ShapeDtypeStruct((rows1 // 4, width...  83.8 us
    unnamed x2, local copies, waits for them, and re-layouts  3.55 us

profile of v3, /device:TPU:1, one launch (start us, length us, event | category | flops | bytes accessed | tf_op | source)
XLA Modules:
  0.0 88.0 jit_solution(1449349391767217897)
XLA Ops:
  0.6 83.8 %layer.1 = (bf16[128,2048]{1,0:T(8,128)(2,1)}, bf16[256,512]{1,0:T(8,128)(2,1)}) custom-call(bf16[512,2048]{1,0:T(8,128)(2,1)} %tok1_h.1, f32[1,2048]{1,0:T(1,128)} %bitcast.5, bf16[2048,128]{1,0:T(8,128)(2,1)} %wq_h.1, bf16[2048,128]{1,0:T(8,128)(2,1)} %wk_h.1, bf16[2048,256]{1,0:T(8,128)(2,1)} %wv_h.1, bf16[2048,256]{1,0:T(8,128)(2,1)} %wo_h.1, ...), custom_call_target="tpu_custom_call" | custom-call | tf_op jit(solution)/shard_map/layer/pallas_call | solution.py:462
  84.4 1.9 %copy.21 = bf16[128,2048]{1,0:T(8,128)(2,1)} copy(bf16[128,2048]{1,0:T(8,128)(2,1)} %get-tuple-element.4) | data formatting | bytes 1048576
  86.3 1.7 %copy.22 = bf16[256,512]{1,0:T(8,128)(2,1)} copy(bf16[256,512]{1,0:T(8,128)(2,1)} %get-tuple-element.5) | data formatting | bytes 524288

commit v4 on v3

--- a/solution.py
+++ b/solution.py
@@ -108,8 +108,8 @@
     for m in (1, 3):
         pl.semaphore_signal(barrier, inc=1, device_id=(ep, flips[m]), device_id_type=MESH)
 
-    for cp in loads:
-        cp.start()
+    for i in (0, 10, 1, 2, 3, 4, 5, 6):
+        loads[i].start()
 
     rows2 = norm2.shape[0]
     experts = send2.shape[0]
@@ -184,6 +184,8 @@
     def handed(n, k):
         remote(wfull.at[0:n], wfull.at[0:n], w_ssem, w_rsem.at[k], ep, tp).wait_recv()
 
+    for i in range(7, 10):
+        loads[i].start()
     loads[10].wait()
     hand_on(tp, 0, 64, 0, ep, flips[1])
     hand_on(tp, 64, 64, 1, ep, flips[3])
@@ -351,7 +353,6 @@
     zmsg[0:64, :], zmsg[64:72, :] = row_state, row_total
     for d in range(1, NZ):
         pl.when(z + d < NZ)(z_share(d).start)
-    pass_on(NEAR, NEAR)
     cols_in = jnp.concatenate(
         [routes_t_ref[...].astype(F32), share_t, jnp.zeros((4, rows2), F32)], axis=0
     )
@@ -367,6 +368,7 @@
         slot = jnp.sum(jnp.where(r_cols[r] == e_lane, rank, 0.0), axis=1, keepdims=True)
         pickm[r] = (lanes == slot + r_cols[r] * CAP).astype(BF16)
 
+    pass_on(NEAR, NEAR)
     reduce(0)
     middle(1)
     arrived(2)
@@ -406,9 +408,6 @@
         gated[rows, :] = (rows_out * (out_gate * jax.nn.sigmoid(out_gate))).astype(BF16)
     quarter = out1_ref.shape[0]
     mine_cols = pl.ds(pl.multiple_of(tp * 256, 256), 256)
-    for m in range(1, 4):
-        rows = pl.ds(pl.multiple_of(flips[m] * quarter, quarter), quarter)
-        remote(gated.at[rows], spread.at[:, mine_cols], mx_ssem, mx_rsem, ep, flips[m]).start()
     spread[:, mine_cols] = gated[pl.ds(pl.multiple_of(tp * quarter, quarter), quarter), :]
 
     arrived(5)
@@ -417,14 +416,17 @@
     reduce(2)
     middle(4)
     middle(5)
+    for m in range(1, 4):
+        rows = pl.ds(pl.multiple_of(flips[m] * quarter, quarter), quarter)
+        remote(gated.at[rows], spread.at[:, mine_cols], mx_ssem, mx_rsem, ep, flips[m]).start()
     reduce(3)
+    reduce(4)
+    reduce(5)
     remote(spread.at[:, 0:768], spread.at[:, 0:768], mx_ssem, mx_rsem, ep, tp).wait_recv()
     handed(384, 4)
     for n in range(4):
         cols = slice(512 * n, 512 * n + 512)
         out1_ref[:, cols] = dot(spread[...], wfull[:, cols]).astype(BF16)
-    reduce(4)
-    reduce(5)
 
     remote(rret.at[1:experts], rret.at[1:experts], rt_ssem, rt_rsem, ep, tp).wait_recv()
     flat = rret[...].reshape(experts * CAP, 512)
@@ -447,6 +449,11 @@
         pl.when(z + d < NZ)(z_share(d).wait_send)
 
 
+def write_out(first_ref, second_ref, out1_ref, out2_ref):
+    out1_ref[...] = first_ref[...]
+    out2_ref[...] = second_ref[...]
+
+
 def body(
     tokens_first, norm_gain_first, w_query, w_key, w_value, w_outgate, w_decay, decay_bias,
     head_gain, w_mix_out, tokens_second, norm_gain_second, routes, route_logits,
@@ -459,7 +466,7 @@
     experts = NZ * NY * NC
     quarter = width // 4
     V, D = pltpu.VMEM, pltpu.SemaphoreType.DMA
-    return pl.pallas_call(
+    first, second = pl.pallas_call(
         kernel,
         out_shape=(
             jax.ShapeDtypeStruct((rows1 // 4, width), BF16),
@@ -501,6 +508,16 @@
         norm_gain_second.reshape(1, -1), routes.T, route_logits.T,
         expert_gate, expert_up, expert_down,
     )
+    return pl.pallas_call(
+        write_out,
+        out_shape=(
+            jax.ShapeDtypeStruct(first.shape, BF16), jax.ShapeDtypeStruct(second.shape, BF16)
+        ),
+        in_specs=[vmem, vmem],
+        out_specs=(vmem, vmem),
+        compiler_params=pltpu.CompilerParams(vmem_limit_bytes=4 * 2**20),
+        name="write_out",
+    )(first, second)
 
 
 def solution(mesh):

time: 88.2 us -> 86 us (0.975)
  local copies, waits for them, and re-layouts: 3.55 us -> 1.98 us
    pallas_call x1, Pallas kernels: 83.8 us -> 82.2 us  [body(): pl.pallas_call(kernel, out_shape=(jax.ShapeDtypeStruct((rows1 // 4, width...]
    unnamed x2 -> x4, local copies, waits for them, and re-layouts: 3.55 us -> 1.98 us
    pallas_call x0 -> x1, Pallas kernels: none -> 0.93 us  [body(): pl.pallas_call(write_out, out_shape=(jax.ShapeDtypeStruct(first.shape, BF...]
where the time goes in v4:
time: 86 us; the launch traced here: 85.8 us
  Pallas kernels  83.1 us (97%)
  local copies, waits for them, and re-layouts  1.98 us (2%)
    pallas_call x1, Pallas kernels, body(): pl.pallas_call(kernel, out_shape=(jax.ShapeDtypeStruct((rows1 // 4, width...  82.2 us
    unnamed x4, local copies, waits for them, and re-layouts  1.98 us

profile of v4, /device:TPU:1, one launch (start us, length us, event | category | flops | bytes accessed | tf_op | source)
XLA Modules:
  0.0 85.8 jit_solution(12669845218949375438)
XLA Ops:
  0.6 82.2 %layer.1 = (bf16[128,2048]{1,0:T(8,128)(2,1)}, bf16[256,512]{1,0:T(8,128)(2,1)}) custom-call(bf16[512,2048]{1,0:T(8,128)(2,1)} %tok1_h.1, f32[1,2048]{1,0:T(1,128)} %bitcast.5, bf16[2048,128]{1,0:T(8,128)(2,1)} %wq_h.1, bf16[2048,128]{1,0:T(8,128)(2,1)} %wk_h.1, bf16[2048,256]{1,0:T(8,128)(2,1)} %wv_h.1, bf16[2048,256]{1,0:T(8,128)(2,1)} %wo_h.1, ...), custom_call_target="tpu_custom_call" | custom-call | tf_op jit(solution)/shard_map/layer/pallas_call | solution.py:469
  82.9 0.0 copy-start
  82.9 1.0 %copy-done = bf16[128,2048]{1,0:T(8,128)(2,1)S(1)} copy-done((bf16[128,2048]{1,0:T(8,128)(2,1)S(1)}, bf16[128,2048]{1,0:T(8,128)(2,1)}, u32[]{:S(2)}) %copy-start) | copy-done | bytes 524312
  83.9 0.0 copy-start.1
  83.9 0.9 %copy-done.1 = bf16[256,512]{1,0:T(8,128)(2,1)S(1)} copy-done((bf16[256,512]{1,0:T(8,128)(2,1)S(1)}, bf16[256,512]{1,0:T(8,128)(2,1)}, u32[]{:S(2)}) %copy-start.1) | copy-done | bytes 262168
  84.8 0.9 %write_out.1 = (bf16[128,2048]{1,0:T(8,128)(2,1)}, bf16[256,512]{1,0:T(8,128)(2,1)}) custom-call(bf16[128,2048]{1,0:T(8,128)(2,1)S(1)} %copy-done, bf16[256,512]{1,0:T(8,128)(2,1)S(1)} %copy-done.1), custom_call_target="tpu_custom_call" | custom-call | tf_op jit(solution)/shard_map/write_out/pallas_call | solution.py:511
Async XLA Ops:
  82.9 1.0 %copy-start = (bf16[128,2048]{1,0:T(8,128)(2,1)S(1)}, bf16[128,2048]{1,0:T(8,128)(2,1)}, u32[]{:S(2)}) copy-start(bf16[128,2048]{1,0:T(8,128)(2,1)} %get-tuple-element.4.first_ref) | copy-start | bytes 1572868
  83.9 0.9 %copy-start.1 = (bf16[256,512]{1,0:T(8,128)(2,1)S(1)}, bf16[256,512]{1,0:T(8,128)(2,1)}, u32[]{:S(2)}) copy-start(bf16[256,512]{1,0:T(8,128)(2,1)} %get-tuple-element.5.second_ref) | copy-start | bytes 786436

commit v5 on v4

--- a/solution.py
+++ b/solution.py
@@ -328,10 +328,6 @@
     pass_on(FAR, FAR)
     pass_on(FAR, NEAR)
     pass_on(NEAR, FAR)
-    handed(128, 2)
-    handed(128, 3)
-    for m in range(1, 4):
-        hand_on(flips[m], 0, 128, 4, partner, tp)
     arrived(1)
     expert(1)
     middle(0)
@@ -371,6 +367,10 @@
     pass_on(NEAR, NEAR)
     reduce(0)
     middle(1)
+    handed(128, 2)
+    handed(128, 3)
+    for m in range(1, 4):
+        hand_on(flips[m], 0, 128, 4, partner, tp)
     arrived(2)
     expert(2)
     reduce(1)

time: 86 us -> 86 us (level)
  no operation moved by 1% of the time
where the time goes in v5:
time: 86 us; the launch traced here: 85.8 us
  Pallas kernels  83.1 us (97%)
  local copies, waits for them, and re-layouts  1.98 us (2%)
    pallas_call x1, Pallas kernels, body(): pl.pallas_call(kernel, out_shape=(jax.ShapeDtypeStruct((rows1 // 4, width...  82.2 us
    unnamed x4, local copies, waits for them, and re-layouts  1.98 us

profile of v5, /device:TPU:1, one launch (start us, length us, event | category | flops | bytes accessed | tf_op | source)
XLA Modules:
  0.0 85.8 jit_solution(4496207709100096001)
XLA Ops:
  0.6 82.2 %layer.1 = (bf16[128,2048]{1,0:T(8,128)(2,1)}, bf16[256,512]{1,0:T(8,128)(2,1)}) custom-call(bf16[512,2048]{1,0:T(8,128)(2,1)} %tok1_h.1, f32[1,2048]{1,0:T(1,128)} %bitcast.5, bf16[2048,128]{1,0:T(8,128)(2,1)} %wq_h.1, bf16[2048,128]{1,0:T(8,128)(2,1)} %wk_h.1, bf16[2048,256]{1,0:T(8,128)(2,1)} %wv_h.1, bf16[2048,256]{1,0:T(8,128)(2,1)} %wo_h.1, ...), custom_call_target="tpu_custom_call" | custom-call | tf_op jit(solution)/shard_map/layer/pallas_call | solution.py:469
  82.9 0.0 copy-start
  82.9 1.0 %copy-done = bf16[128,2048]{1,0:T(8,128)(2,1)S(1)} copy-done((bf16[128,2048]{1,0:T(8,128)(2,1)S(1)}, bf16[128,2048]{1,0:T(8,128)(2,1)}, u32[]{:S(2)}) %copy-start) | copy-done | bytes 524312
  83.9 0.0 copy-start.1
  83.9 0.9 %copy-done.1 = bf16[256,512]{1,0:T(8,128)(2,1)S(1)} copy-done((bf16[256,512]{1,0:T(8,128)(2,1)S(1)}, bf16[256,512]{1,0:T(8,128)(2,1)}, u32[]{:S(2)}) %copy-start.1) | copy-done | bytes 262168
  84.8 0.9 %write_out.1 = (bf16[128,2048]{1,0:T(8,128)(2,1)}, bf16[256,512]{1,0:T(8,128)(2,1)}) custom-call(bf16[128,2048]{1,0:T(8,128)(2,1)S(1)} %copy-done, bf16[256,512]{1,0:T(8,128)(2,1)S(1)} %copy-done.1), custom_call_target="tpu_custom_call" | custom-call | tf_op jit(solution)/shard_map/write_out/pallas_call | solution.py:511
Async XLA Ops:
  82.9 1.0 %copy-start = (bf16[128,2048]{1,0:T(8,128)(2,1)S(1)}, bf16[128,2048]{1,0:T(8,128)(2,1)}, u32[]{:S(2)}) copy-start(bf16[128,2048]{1,0:T(8,128)(2,1)} %get-tuple-element.4.first_ref) | copy-start | bytes 1572868
  83.9 0.9 %copy-start.1 = (bf16[256,512]{1,0:T(8,128)(2,1)S(1)}, bf16[256,512]{1,0:T(8,128)(2,1)}, u32[]{:S(2)}) copy-start(bf16[256,512]{1,0:T(8,128)(2,1)} %get-tuple-element.5.second_ref) | copy-start | bytes 786436
